TPU v7x, 32 devices: a whole 2x2x4 slice. The times are simulated.
32 devices in a mesh: sp: 16 (over z, y, x), tp: 2 (over core).
Axes of the slice: x: 2, y: 2, z: 4, core: 2. Of those that a mesh axis runs over, the one named last changes fastest.
Arguments:
- queries: bfloat16 [4096, 1024], P('sp', 'tp'), may hold values from -6 to 6
- key_vectors: bfloat16 [4096, 1024], P('sp', 'tp'), may hold values from -6 to 6
- value_vectors: bfloat16 [4096, 1024], P('sp', 'tp'), may hold values from -6 to 6
- gate_inputs: bfloat16 [4096, 1024], P('sp', 'tp'), may hold values from -6 to 6
- log_decay: float32 [4096, 16], P('sp', 'tp'), may hold values from -1 to 0
- head_gain: float32 [1024], P('tp'), may hold values from 0.1 to 1.9
- out_weight: bfloat16 [1024, 2048], P('tp'), may hold values from -0.1875 to 0.1875
- residual: bfloat16 [4096, 2048], P(('sp', 'tp')), may hold values from -6 to 6
- norm_gain: float32 [2048], replicated, may hold values from 0.1 to 1.9
- expert_ids: int32 [4096, 2], P(('sp', 'tp')), may hold values from 0 to 15, all different within a row; in each aligned block of 128 rows (0 to 127, 128 to 255, ...) at most 32 rows name the same one
- expert_weights: float32 [4096, 2], P(('sp', 'tp')), may hold values from 0.2 to 1
- gate_experts: bfloat16 [16, 2048, 3584], P('sp', None, 'tp'), may hold values from -0.125 to 0.125
- up_experts: bfloat16 [16, 2048, 3584], P('sp', None, 'tp'), may hold values from -0.125 to 0.125
- down_experts: bfloat16 [16, 3584, 2048], P('sp', 'tp'), may hold values from -0.09375 to 0.09375
Outputs:
- layer_out: bfloat16 [4096, 2048], P(('sp', 'tp'))
Inputs may be any that keep to these rules, and one draw needn't show every extreme that they name: `expert_ids`: the 2 experts of a token differ. No expert is named more than 32 times in the rows of one device, and in some device some expert is named exactly 32 times.
All inputs are finite; a program needn't handle non-finite values.
Results may differ from a plain program's by a relative error of at most 0.014.
Values may be sent and summed in bfloat16 or wider, within the bound.
A program may use at most 128 MiB of HBM per device.

v0:
```python
import jax
import jax.numpy as jnp
from jax import lax
from jax.sharding import PartitionSpec as P


def swap(value):
    return lax.ppermute(value, "tp", [(0, 1), (1, 0)])


def incoming_state(total, state):
    heads, size, _ = state.shape
    count = lax.axis_size("sp")
    state = jnp.swapaxes(state, 0, 1).reshape(size, heads * size)
    total = jnp.repeat(total, size)[None, :]

    def shift(total, state, distance):
        high = total.astype(jnp.bfloat16)
        low = (total - high.astype(jnp.float32)).astype(jnp.bfloat16)
        packed = jnp.concatenate([state.astype(jnp.bfloat16), high, low], axis=0)
        got = lax.ppermute(packed, "sp", [(i, i + distance) for i in range(count - distance)])
        got = got.astype(jnp.float32)
        return got[size : size + 1] + got[size + 1 : size + 2], got[:size]

    before_total, before_state = jnp.zeros_like(total), jnp.zeros_like(state)
    distance = 1
    while distance < count:
        earlier_total, earlier_state = shift(total, state, distance)
        before_state = jnp.exp(before_total) * earlier_state + before_state
        before_total = before_total + earlier_total
        state = jnp.exp(total) * earlier_state + state
        total = total + earlier_total
        distance *= 2
    return jnp.swapaxes(before_state.reshape(size, heads, size), 0, 1)


def rotate(block, places):
    half_size = block.shape[-1] // 2
    frequency = 10000.0 ** (-jnp.arange(half_size, dtype=jnp.float32) / half_size)
    angles = places.astype(jnp.float32)[:, None, None] * frequency
    first_half = block[..., :half_size]
    second = block[..., half_size:]
    return jnp.concatenate(
        [
            first_half * jnp.cos(angles) - second * jnp.sin(angles),
            second * jnp.cos(angles) + first_half * jnp.sin(angles),
        ],
        axis=-1,
    )


def expert_hidden(batch, gate_matrix, up_matrix):
    gate_value = jnp.dot(batch, gate_matrix, preferred_element_type=jnp.float32)
    up_value = jnp.dot(batch, up_matrix, preferred_element_type=jnp.float32)
    return (jax.nn.silu(gate_value) * up_value).astype(jnp.bfloat16)


def shards(
    queries,
    key_vectors,
    value_vectors,
    gate_inputs,
    log_decay,
    head_gain,
    out_weight,
    residual,
    norm_gain,
    expert_ids,
    expert_weights,
    gate_experts,
    up_experts,
    down_experts,
):
    tok_dev, channels = queries.shape
    head_count = log_decay.shape[1]
    head_size = channels // head_count
    places = lax.axis_index("sp") * tok_dev + jnp.arange(tok_dev, dtype=jnp.int32)
    core = lax.axis_index("tp")
    turned_queries = rotate(
        queries.astype(jnp.float32).reshape(tok_dev, head_count, head_size), places
    )
    turned_keys = rotate(
        key_vectors.astype(jnp.float32).reshape(tok_dev, head_count, head_size), places
    ) * head_size ** (-0.5)
    value_float = value_vectors.astype(jnp.float32).reshape(tok_dev, head_count, head_size)
    running = jnp.cumsum(log_decay, axis=0)
    device_total = running[-1]
    end_weight = jnp.exp(device_total[None, :] - running)
    local_end = jnp.einsum(
        "thd,the->hde",
        turned_keys * end_weight[:, :, None],
        value_float,
        precision=lax.Precision.HIGH,
    )
    incoming = incoming_state(device_total, local_end)
    by_head = running.T
    log_gaps = by_head[:, :, None] - by_head[:, None, :]
    offsets = jnp.arange(tok_dev)
    causal = offsets[:, None] >= offsets[None, :]
    decay_weight = jnp.where(causal, jnp.exp(jnp.where(causal, log_gaps, 0.0)), 0.0)
    scores = (
        jnp.einsum("thd,shd->hts", turned_queries, turned_keys, precision=lax.Precision.HIGH)
        * decay_weight
    )
    within = jnp.einsum("hts,she->the", scores, value_float, precision=lax.Precision.HIGH)
    carried = jnp.einsum(
        "thd,hde->the",
        turned_queries * jnp.exp(running)[:, :, None],
        incoming,
        precision=lax.Precision.HIGH,
    )
    retained = within + carried
    squares = jnp.mean(retained * retained, axis=-1, keepdims=True)
    normed = retained * lax.rsqrt(squares + 1e-06) * head_gain.reshape(head_count, head_size)
    normed = (
        normed.reshape(tok_dev, channels) * jax.nn.silu(gate_inputs.astype(jnp.float32))
    ).astype(jnp.bfloat16)
    half = tok_dev // 2
    normed_away = lax.dynamic_slice_in_dim(normed, (1 - core) * half, half, 0)
    normed_here = lax.dynamic_slice_in_dim(normed, core * half, half, 0)
    away = jnp.dot(normed_away, out_weight, preferred_element_type=jnp.float32)
    got = swap(away.astype(jnp.bfloat16))
    here = jnp.dot(normed_here, out_weight, preferred_element_type=jnp.float32)
    projected = here.astype(jnp.bfloat16).astype(jnp.float32) + got.astype(jnp.float32)
    mixed_rows = (residual.astype(jnp.float32) + projected).astype(jnp.bfloat16)
    mixed_float = mixed_rows.astype(jnp.float32)
    normed_rows = (
        mixed_float
        * lax.rsqrt(jnp.mean(mixed_float * mixed_float, axis=-1, keepdims=True) + 1e-06)
        * norm_gain
    ).astype(jnp.bfloat16)
    d_model = residual.shape[1]
    experts = lax.axis_size("sp")
    capacity = 2 * tok_dev // experts
    slots = experts * capacity
    top_count = expert_ids.shape[1]
    flat_routes = expert_ids.reshape(-1)
    onehot = (flat_routes[:, None] == jnp.arange(experts, dtype=jnp.int32)[None, :]).astype(
        jnp.int32
    )
    slot_rank = jnp.sum(jnp.cumsum(onehot, axis=0) * onehot, axis=1) - 1
    slot = (flat_routes * capacity + slot_rank).reshape(-1, top_count)
    every_slot = jnp.arange(slots, dtype=jnp.int32)
    place = jnp.zeros((slots, half), jnp.bool_)
    weigh = jnp.zeros((half, slots), jnp.float32)
    for choice in range(top_count):
        column = slot[:, choice]
        place = place | (every_slot[:, None] == column[None, :])
        weigh = weigh + jnp.where(
            column[:, None] == every_slot[None, :], expert_weights[:, choice][:, None], 0.0
        )
    outgoing = jnp.dot(
        place.astype(jnp.bfloat16), normed_rows, preferred_element_type=jnp.float32
    ).astype(jnp.bfloat16)
    arrived = lax.all_to_all(
        outgoing.reshape(experts, capacity, d_model), "sp", split_axis=0, concat_axis=0, tiled=True
    ).reshape(slots, d_model)
    both = jnp.concatenate([swap(arrived), arrived], axis=0)
    hidden = expert_hidden(both, gate_experts[0], up_experts[0])
    part = jnp.dot(hidden, down_experts[0], preferred_element_type=jnp.float32).astype(
        jnp.bfloat16
    )
    got_part = swap(part[:slots])
    part_here = part[slots:]
    summed = (
        part_here.astype(jnp.float32) + got_part.astype(jnp.float32)
    ).astype(jnp.bfloat16)
    returned = lax.all_to_all(
        summed.reshape(experts, capacity, d_model), "sp", split_axis=0, concat_axis=0, tiled=True
    ).reshape(slots, d_model)
    weigh_high = weigh.astype(jnp.bfloat16)
    weigh_low = (weigh - weigh_high.astype(jnp.float32)).astype(jnp.bfloat16)
    expert_sum = jnp.dot(weigh_high, returned, preferred_element_type=jnp.float32) + jnp.dot(
        weigh_low, returned, preferred_element_type=jnp.float32
    )
    return (mixed_float + expert_sum).astype(jnp.bfloat16)


def solution(mesh):
    return jax.shard_map(
        shards,
        mesh=mesh,
        in_specs=(
            P("sp", "tp"),
            P("sp", "tp"),
            P("sp", "tp"),
            P("sp", "tp"),
            P("sp", "tp"),
            P("tp"),
            P("tp", None),
            P(("sp", "tp"), None),
            P(),
            P(("sp", "tp"), None),
            P(("sp", "tp"), None),
            P("sp", None, "tp"),
            P("sp", None, "tp"),
            P("sp", "tp", None),
        ),
        out_specs=P(("sp", "tp"), None),
        check_vma=False,
    )
```

profile of v0, /device:TPU:14, one launch (start us, length us, event | category | flops | bytes accessed | tf_op | source)
XLA Modules:
  0.0 205.6 jit_solution(7099621895362893546)
XLA Ops:
  0.0 1.4 reduce-window.14
  7.6 1.3 multiply_subtract_fusion.1
  10.4 3.4 %collective-permute-start = (bf16[66,512]{1,0:T(8,128)(2,1)S(1)}, bf16[66,512]{1,0:T(8,128)(2,1)S(1)}, u32[]{:S(2)}, u32[]{:S(2)}) collective-permute-start(bf16[66,512]{1,0:T(8,128)(2,1)S(1)} %pad_maximum_fusion.9), channel_id=1, source_target_pairs={{0,2},{2,4},{4,6},{6,8},{8,10},{10,12},{12,14},{14,16},{16,18},{18... | collective-permute-start | bytes 202760 | tf_op jit(solution)/shard_map/ppermute | solution.py:21
  15.7 2.9 %fusion.19 = f32[256,8,64]{0,2,1:T(8,128)} fusion(bf16[256,8,64]{0,2,1:T(8,128)(2,1)} %bitcast.86, f32[8,256,256]{2,1,0:T(8,128)S(1)} %fusion.39, f32[8,256]{1,0:T(8,128)S(1)} %add_bitcast_fusion.2, pred[256,256]{1,0:T(8,128)(4,1)S(1)} %iota_compare_fusion.4), kind=kOutput, calls=%fused_computation.26 | convolution fusion | flops 203423744 | bytes 2957312 | tf_op jit(solution)/shard_map/hts,she->the/dot_general | solution.py:105
  19.2 3.4 %collective-permute-start.1 = (bf16[66,512]{1,0:T(8,128)(2,1)S(1)}, bf16[66,512]{1,0:T(8,128)(2,1)S(1)}, u32[]{:S(2)}, u32[]{:S(2)}) collective-permute-start(bf16[66,512]{1,0:T(8,128)(2,1)S(1)} %pad_maximum_fusion.10), channel_id=1, source_target_pairs={{0,4},{2,6},{4,8},{6,10},{8,12},{10,14},{12,16},{14,18},{16,20},{1... | collective-permute-start | bytes 202760 | tf_op jit(solution)/shard_map/ppermute | solution.py:21
  23.4 2.0 collective-permute-done.1
  25.5 3.5 %collective-permute-start.2 = (bf16[66,512]{1,0:T(8,128)(2,1)S(1)}, bf16[66,512]{1,0:T(8,128)(2,1)S(1)}, u32[]{:S(2)}, u32[]{:S(2)}) collective-permute-start(bf16[66,512]{1,0:T(8,128)(2,1)S(1)} %pad_maximum_fusion.11), channel_id=1, source_target_pairs={{0,8},{2,10},{4,12},{6,14},{8,16},{10,18},{12,20},{14,22},{16,24},... | collective-permute-start | bytes 202760 | tf_op jit(solution)/shard_map/ppermute | solution.py:21
  29.2 2.5 %collective-permute-done.2 = bf16[66,512]{1,0:T(8,128)(2,1)S(1)} collective-permute-done((bf16[66,512]{1,0:T(8,128)(2,1)S(1)}, bf16[66,512]{1,0:T(8,128)(2,1)S(1)}, u32[]{:S(2)}, u32[]{:S(2)}) %collective-permute-start.2) | collective-permute-done | bytes 67616 | tf_op jit(solution)/shard_map/ppermute | solution.py:21
  31.9 3.0 %collective-permute-start.3 = (bf16[66,512]{1,0:T(8,128)(2,1)S(1)}, bf16[66,512]{1,0:T(8,128)(2,1)S(1)}, u32[]{:S(2)}, u32[]{:S(2)}) collective-permute-start(bf16[66,512]{1,0:T(8,128)(2,1)S(1)} %pad_maximum_fusion.12), channel_id=1, source_target_pairs={{0,16},{2,18},{4,20},{6,22},{8,24},{10,26},{12,28},{14,30},{1,17},... | collective-permute-start | bytes 202760 | tf_op jit(solution)/shard_map/ppermute | solution.py:21
  34.9 1.9 collective-permute-done.3
  37.0 1.4 multiply_reduce_fusion
  40.7 1.7 collective-permute-done.4
  42.4 1.7 fusion.23
  44.9 56.8 %all_to_all.10 = bf16[16,32,2048]{2,1,0:T(8,128)(2,1)S(1)} all-to-all(bf16[16,32,2048]{2,1,0:T(8,128)(2,1)S(1)} %bitcast.77), channel_id=1, replica_groups=mesh['sp'=16,'tp'=2] {'sp'}, dimensions={0} | all-to-all | bytes 4194304 | tf_op jit(solution)/shard_map/all_to_all | solution.py:155
  101.7 4.2 %collective-permute-done.5 = bf16[512,2048]{1,0:T(8,128)(2,1)S(1)} collective-permute-done((bf16[512,2048]{1,0:T(8,128)(2,1)S(1)}, bf16[512,2048]{1,0:T(8,128)(2,1)S(1)}, u32[]{:S(2)}, u32[]{:S(2)}) %collective-permute-start.5) | collective-permute-done | bytes 2097184 | tf_op jit(solution)/shard_map/ppermute | solution.py:8
  105.8 11.0 %fusion.4 = f32[1024,1792]{1,0:T(8,128)S(1)} fusion(bf16[1,2048,1792]{2,1,0:T(8,128)(2,1)} %param.25, bf16[512,2048]{1,0:T(8,128)(2,1)S(1)} %bitcast.79, bf16[512,2048]{1,0:T(8,128)(2,1)S(1)} %collective-permute-done.5), kind=kOutput, calls=%fused_computation.4 | convolution fusion | flops 7524581376 | bytes 18874368 | tf_op jit(solution)/shard_map/dot_general | solution.py:53
  116.8 11.4 %fusion.2 = f32[1024,1792]{1,0:T(8,128)} fusion(bf16[1,2048,1792]{2,1,0:T(8,128)(2,1)S(1)} %bitcast.94, bf16[512,2048]{1,0:T(8,128)(2,1)S(1)} %bitcast.80, bf16[512,2048]{1,0:T(8,128)(2,1)S(1)} %collective-permute-done.5), kind=kOutput, calls=%fused_computation.2 | convolution fusion | flops 7524581376 | bytes 18874368 | tf_op jit(solution)/shard_map/dot_general | solution.py:54
  128.3 10.6 %fusion.6 = bf16[1024,2048]{1,0:T(8,128)(2,1)S(1)} fusion(bf16[1,1792,2048]{2,1,0:T(8,128)(2,1)S(1)} %bitcast.96, f32[1024,1792]{1,0:T(8,128)} %fusion.2, f32[1024,1792]{1,0:T(8,128)S(1)} %fusion.4), kind=kOutput, calls=%fused_computation.9 | convolution fusion | flops 7529299968 | bytes 26214400 | tf_op jit(solution)/shard_map/dot_general | solution.py:160
  139.3 4.0 %collective-permute-done.6 = bf16[512,2048]{1,0:T(8,128)(2,1)S(1)} collective-permute-done((bf16[512,2048]{1,0:T(8,128)(2,1)S(1)}, bf16[512,2048]{1,0:T(8,128)(2,1)S(1)}, u32[]{:S(2)}, u32[]{:S(2)}) %collective-permute-start.6) | collective-permute-done | bytes 2097184 | tf_op jit(solution)/shard_map/ppermute | solution.py:8
  143.4 2.1 %add_convert_fusion = bf16[512,2048]{1,0:T(8,128)(2,1)} fusion(bf16[512,2048]{1,0:T(8,128)(2,1)S(1)} %collective-permute-done.6, bf16[1024,2048]{1,0:T(8,128)(2,1)S(1)} %fusion.6), kind=kLoop, calls=%fused_computation.8 | loop fusion | flops 4194304 | bytes 6291456 | tf_op jit(solution)/shard_map/convert_element_type | solution.py:167
  145.5 6.4 %all-to-all-start.1 = ((bf16[16,32,2048]{2,1,0:T(8,128)(2,1)}), bf16[16,32,2048]{2,1,0:T(8,128)(2,1)}, u32[]{:S(2)}, u32[]{:S(2)}) async-start(bf16[16,32,2048]{2,1,0:T(8,128)(2,1)} %bitcast.76), calls=%async_computation.1 | async-start | bytes 4194304 | tf_op jit(solution)/shard_map/all_to_all | solution.py:168
  151.9 48.7 %all-to-all-done.1 = bf16[16,32,2048]{2,1,0:T(8,128)(2,1)} async-done(((bf16[16,32,2048]{2,1,0:T(8,128)(2,1)}), bf16[16,32,2048]{2,1,0:T(8,128)(2,1)}, u32[]{:S(2)}, u32[]{:S(2)}) %all-to-all-start.1) | async-done | bytes 2097184 | tf_op jit(solution)/shard_map/all_to_all | solution.py:168
  200.6 2.1 %fusion.48 = f32[128,2048]{1,0:T(8,128)S(1)} fusion(bf16[512,2048]{1,0:T(8,128)(2,1)} %bitcast.32, f32[128]{0:T(128)S(1)} %get-tuple-element.36, s32[128]{0:T(128)S(1)} %get-tuple-element.38, f32[128]{0:T(128)S(1)} %get-tuple-element.35, s32[128]{0:T(128)S(1)} %get-tuple-element.37), kind=kOutput, calls=%fused_computation.71 | convolution fusion | flops 269025280 | bytes 3147776 | tf_op jit(solution)/shard_map/dot_general | solution.py:173
  202.7 2.9 %fusion.11 = bf16[128,2048]{1,0:T(8,128)(2,1)} fusion(f32[128,2048]{1,0:T(8,128)S(1)} %fusion.48, bf16[512,2048]{1,0:T(8,128)(2,1)} %bitcast.32, bf16[128,2048]{1,0:T(8,128)(2,1)S(1)} %get-tuple-element.42, f32[128]{0:T(128)S(1)} %get-tuple-element.36, s32[128]{0:T(128)S(1)} %get-tuple-element.38, f32[128]{0:T(128)S(1)} %get-tuple-element.35, ...), kind=kOutput, calls=%fused_computation.14 | convolution fusion | flops 269877248 | bytes 4196352 | tf_op jit(solution)/shard_map/dot_general | solution.py:173
  (103 shorter events, 14.8 us)
Async XLA Ops:
  0.0 39.9 %copy-start = (bf16[512,2048]{1,0:T(8,128)(2,1)S(1)}, bf16[512,2048]{1,0:T(8,128)(2,1)}, u32[]{:S(2)}) copy-start(bf16[512,2048]{1,0:T(8,128)(2,1)} %param.20) | copy-start | bytes 6291460
  1.6 0.6 copy-start.3
  2.4 6.9 %copy-start.5 = (f32[8]{0:T(128)}, f32[8]{0:T(128)S(1)}, u32[]{:S(2)}) copy-start(f32[8]{0:T(128)S(1)} %slice_reduce_fusion.2) | copy-start | bytes 100
  7.4 1.6 copy-start.2
  9.6 9.0 %copy-start.6 = (f32[8]{0:T(128)S(1)}, f32[8]{0:T(128)}, u32[]{:S(2)}) copy-start(f32[8]{0:T(128)} %copy-done.5) | copy-start | bytes 100
  9.6 9.2 %copy-start.7 = (s32[128,2]{0,1:T(2,128)S(1)}, s32[128,2]{0,1:T(2,128)}, u32[]{:S(2)}) copy-start(s32[128,2]{0,1:T(2,128)} %param.23) | copy-start | bytes 3076
  10.4 8.6 %collective-permute-start = (bf16[66,512]{1,0:T(8,128)(2,1)S(1)}, bf16[66,512]{1,0:T(8,128)(2,1)S(1)}, u32[]{:S(2)}, u32[]{:S(2)}) collective-permute-start(bf16[66,512]{1,0:T(8,128)(2,1)S(1)} %pad_maximum_fusion.9), channel_id=1, source_target_pairs={{0,2},{2,4},{4,6},{6,8},{8,10},{10,12},{12,14},{14,16},{16,18},{18... | collective-permute-start | bytes 202760 | tf_op jit(solution)/shard_map/ppermute | solution.py:21
  14.6 8.1 %copy-start.8 = (f32[512]{0:T(512)S(1)}, f32[512]{0:T(512)}, u32[]{:S(2)}) copy-start(f32[512]{0:T(512)} %param.19) | copy-start | bytes 6148
  19.2 6.2 %collective-permute-start.1 = (bf16[66,512]{1,0:T(8,128)(2,1)S(1)}, bf16[66,512]{1,0:T(8,128)(2,1)S(1)}, u32[]{:S(2)}, u32[]{:S(2)}) collective-permute-start(bf16[66,512]{1,0:T(8,128)(2,1)S(1)} %pad_maximum_fusion.10), channel_id=1, source_target_pairs={{0,4},{2,6},{4,8},{6,10},{8,12},{10,14},{12,16},{14,18},{16,20},{1... | collective-permute-start | bytes 202760 | tf_op jit(solution)/shard_map/ppermute | solution.py:21
  25.5 6.2 %collective-permute-start.2 = (bf16[66,512]{1,0:T(8,128)(2,1)S(1)}, bf16[66,512]{1,0:T(8,128)(2,1)S(1)}, u32[]{:S(2)}, u32[]{:S(2)}) collective-permute-start(bf16[66,512]{1,0:T(8,128)(2,1)S(1)} %pad_maximum_fusion.11), channel_id=1, source_target_pairs={{0,8},{2,10},{4,12},{6,14},{8,16},{10,18},{12,20},{14,22},{16,24},... | collective-permute-start | bytes 202760 | tf_op jit(solution)/shard_map/ppermute | solution.py:21
  31.9 5.0 %collective-permute-start.3 = (bf16[66,512]{1,0:T(8,128)(2,1)S(1)}, bf16[66,512]{1,0:T(8,128)(2,1)S(1)}, u32[]{:S(2)}, u32[]{:S(2)}) collective-permute-start(bf16[66,512]{1,0:T(8,128)(2,1)S(1)} %pad_maximum_fusion.12), channel_id=1, source_target_pairs={{0,16},{2,18},{4,20},{6,22},{8,24},{10,26},{12,28},{14,30},{1,17},... | collective-permute-start | bytes 202760 | tf_op jit(solution)/shard_map/ppermute | solution.py:21
  38.6 5.5 %copy-start.4 = (f32[2048]{0:T(1024)S(1)}, f32[2048]{0:T(1024)}, u32[]{:S(2)}) copy-start(f32[2048]{0:T(1024)} %param.22) | copy-start | bytes 24580
  40.4 2.0 collective-permute-start.4
  101.7 15.1 %slice-start = ((s8[7340032]{0:T(1024)(128)(4,1)}), s8[4194304]{0:T(1024)(128)(4,1)S(1)}, s32[]{:S(2)}) async-start(s8[7340032]{0:T(1024)(128)(4,1)} %bitcast.93), calls=%async_computation.2 | async-start | bytes 8388608
  101.7 15.1 %slice-start.1 = ((s8[7340032]{0:T(1024)(128)(4,1)}), s8[3145728]{0:T(1024)(128)(4,1)S(1)}, s32[]{:S(2)}) async-start(s8[7340032]{0:T(1024)(128)(4,1)} %bitcast.93), calls=%async_computation.3 | async-start | bytes 6291456
  101.7 4.2 %collective-permute-start.5 = (bf16[512,2048]{1,0:T(8,128)(2,1)S(1)}, bf16[512,2048]{1,0:T(8,128)(2,1)S(1)}, u32[]{:S(2)}, u32[]{:S(2)}) collective-permute-start(bf16[512,2048]{1,0:T(8,128)(2,1)S(1)} %bitcast.78), channel_id=1, source_target_pairs={{0,1},{1,0},{2,3},{3,2},{4,5},{5,4},{6,7},{7,6},{8,9},{9,8},{10,11... | collective-permute-start | bytes 6291464 | tf_op jit(solution)/shard_map/ppermute | solution.py:8
  105.8 22.5 %slice-start.2 = ((s8[7340032]{0:T(1024)(128)(4,1)}), s8[4194304]{0:T(1024)(128)(4,1)S(1)}, s32[]{:S(2)}) async-start(s8[7340032]{0:T(1024)(128)(4,1)} %bitcast.95), calls=%async_computation.4 | async-start | bytes 8388608
  116.8 11.5 %slice-start.3 = ((s8[7340032]{0:T(1024)(128)(4,1)}), s8[3145728]{0:T(1024)(128)(4,1)S(1)}, s32[]{:S(2)}) async-start(s8[7340032]{0:T(1024)(128)(4,1)} %bitcast.95), calls=%async_computation.5 | async-start | bytes 6291456
  139.1 12.7 %copy-start.9 = (f32[128,2]{0,1:T(2,128)S(1)}, f32[128,2]{0,1:T(2,128)}, u32[]{:S(2)}) copy-start(f32[128,2]{0,1:T(2,128)} %param.24) | copy-start | bytes 3076
  139.1 4.2 %collective-permute-start.6 = (bf16[512,2048]{1,0:T(8,128)(2,1)S(1)}, bf16[512,2048]{1,0:T(8,128)(2,1)S(1)}, u32[]{:S(2)}, u32[]{:S(2)}) collective-permute-start(bf16[512,2048]{1,0:T(8,128)(2,1)S(1)} %slice.122), channel_id=1, source_target_pairs={{0,1},{1,0},{2,3},{3,2},{4,5},{5,4},{6,7},{7,6},{8,9},{9,8},{10,11... | collective-permute-start | bytes 6291464 | tf_op jit(solution)/shard_map/ppermute | solution.py:8
  145.5 55.1 %all-to-all-start.1 = ((bf16[16,32,2048]{2,1,0:T(8,128)(2,1)}), bf16[16,32,2048]{2,1,0:T(8,128)(2,1)}, u32[]{:S(2)}, u32[]{:S(2)}) async-start(bf16[16,32,2048]{2,1,0:T(8,128)(2,1)} %bitcast.76), calls=%async_computation.1 | async-start | bytes 4194304 | tf_op jit(solution)/shard_map/all_to_all | solution.py:168
  151.8 53.8 %copy-start.1 = (bf16[512,2048]{1,0:T(8,128)(2,1)S(1)}, bf16[512,2048]{1,0:T(8,128)(2,1)}, u32[]{:S(2)}) copy-start(bf16[512,2048]{1,0:T(8,128)(2,1)} %param.20) | copy-start | bytes 6291460
where the time goes:
time: 206 us
  waiting for transfers between devices  65 us (32%)
  blocking collectives  56.8 us (28%)
  matrix products  46.7 us (23%)
  starting transfers between devices  19.9 us (10%)
  other arithmetic  9.98 us (5%)
  local copies, waits for them, and re-layouts  6.8 us (3%)
    all_to_all x1, blocking collectives, shards(): lax.all_to_all(outgoing.reshape(experts, capacity, d_model), 'sp', split_...  56.8 us
    all_to_all x1, waiting for transfers between devices, shards(): lax.all_to_all(summed.reshape(experts, capacity, d_model), 'sp', split_ax...  48.7 us
    ppermute x4, starting transfers between devices, shift(): lax.ppermute(packed, 'sp', [(i, i + distance) for i in range(count - dist...  13.3 us
    dot_general x1, matrix products, expert_hidden(): up_value = jnp.dot(batch, up_matrix, preferred_element_type=jnp.float32)  11.4 us
    dot_general x1, matrix products, expert_hidden(): gate_value = jnp.dot(batch, gate_matrix, preferred_element_type=jnp.float32)  11 us
    dot_general x1, matrix products, shards(): jnp.dot(hidden, down_experts[0], preferred_element_type=jnp.float32)  10.6 us
    ppermute x3, waiting for transfers between devices, swap(): return lax.ppermute(value, 'tp', [(0, 1), (1, 0)])  9.82 us
    ppermute x4, waiting for transfers between devices, shift(): lax.ppermute(packed, 'sp', [(i, i + distance) for i in range(count - dist...  6.41 us
  transfers between devices with their start and end apart: 8, of which 7 were waited for; matrix products, arithmetic and copies ran while one was open for 3% of the time, Pallas kernels for 0%

commit v1 on v0

--- a/solution.py
+++ b/solution.py
@@ -1,7 +1,20 @@
+import functools
+
 import jax
 import jax.numpy as jnp
 from jax import lax
+from jax.experimental import pallas as pl
+from jax.experimental.pallas import tpu as pltpu
 from jax.sharding import PartitionSpec as P
+
+MESH = pl.DeviceIdType.MESH
+
+
+def line_length(count):
+    size = 1
+    while size * size * size < count:
+        size *= 2
+    return size
 
 
 def swap(value):
@@ -49,10 +62,398 @@
     )
 
 
-def expert_hidden(batch, gate_matrix, up_matrix):
-    gate_value = jnp.dot(batch, gate_matrix, preferred_element_type=jnp.float32)
-    up_value = jnp.dot(batch, up_matrix, preferred_element_type=jnp.float32)
-    return (jax.nn.silu(gate_value) * up_value).astype(jnp.bfloat16)
+def experts_kernel(
+    line,
+    plane,
+    cap,
+    parts,
+    chain,
+    rows_ref,
+    mixed_ref,
+    meta_ref,
+    gate_hbm,
+    up_hbm,
+    down_hbm,
+    out_ref,
+    gate_ref,
+    up_ref,
+    down_ref,
+    zbuf,
+    meta,
+    sel,
+    xbuf,
+    hidden,
+    ybuf,
+    yin,
+    sbuf,
+    rbuf,
+    cbuf,
+    csend,
+    pin,
+    wsem,
+    zsend,
+    zrecv,
+    msend,
+    mrecv,
+    psend,
+    precv,
+    tsend,
+    trecv,
+    ysend,
+    yrecv,
+    rsend,
+    rrecv,
+    ssend,
+    srecv,
+):
+    sp, core = lax.axis_index("sp"), lax.axis_index("tp")
+    z, p = sp // plane, lax.rem(sp, plane)
+    tokens, width = rows_ref.shape
+    slots = plane * cap
+    f32, bf16 = jnp.float32, jnp.bfloat16
+
+    def at(line_place, plane_place):
+        return {"sp": line_place * plane + plane_place, "tp": core}
+
+    partner = {"sp": sp, "tp": 1 - core}
+
+    def remote(src, dst, send, recv, device):
+        return pltpu.make_async_remote_copy(
+            src_ref=src,
+            dst_ref=dst,
+            send_sem=send,
+            recv_sem=recv,
+            device_id=device,
+            device_id_type=MESH,
+        )
+
+    weights = []
+    for number, (source, target) in enumerate(
+        ((gate_hbm, gate_ref), (up_hbm, up_ref), (down_hbm, down_ref))
+    ):
+        depth = target.shape[0] // 4
+        for piece in range(4):
+            part = pl.ds(piece * depth, depth)
+            weights.append(
+                pltpu.make_async_copy(
+                    source.at[0, part], target.at[part], wsem.at[number, piece]
+                )
+            )
+
+    barrier = pltpu.get_barrier_semaphore()
+    peers = [at(lax.rem(z + i, line), p) for i in range(1, line)]
+    peers += [at(z, lax.rem(p + i, plane)) for i in range(1, plane)] + [partner]
+    for peer in peers:
+        pl.semaphore_signal(barrier, inc=1, device_id=peer, device_id_type=MESH)
+    for copy in weights:
+        copy.start()
+    pl.semaphore_wait(barrier, len(peers))
+
+    piece_rows = tokens // parts
+    chain_rows = tokens // chain
+
+    def row_copy(way, block, part, target, source=None):
+        rows = pl.ds(part * piece_rows, piece_rows)
+        source = zbuf.at[block] if source is None else source
+        return remote(
+            source.at[rows],
+            zbuf.at[block, rows],
+            zsend.at[way, block, part],
+            zrecv.at[block, part],
+            at(target, p),
+        )
+
+    def meta_copy(i):
+        return remote(
+            meta_ref, meta.at[z], msend.at[i], mrecv.at[i], at(lax.rem(z + i, line), p)
+        )
+
+    for i in range(1, line):
+        meta_copy(i).start()
+    for part in range(parts):
+
+        @pl.when(z + 1 < line)
+        def _():
+            row_copy(0, z, part, z + 1, rows_ref).start()
+
+        @pl.when(z > 0)
+        def _():
+            row_copy(1, z, part, z - 1, rows_ref).start()
+
+    meta[z] = meta_ref[...]
+
+    near = jnp.minimum(z, line - 1 - z)
+    longer_up = z < line - 1 - z
+
+    def block_of(place):
+        both = place <= 2 * near
+        away = jnp.where(both, (place + 1) // 2, place - near)
+        forward = jnp.where(both, place % 2 == 1, longer_up)
+        return jnp.where(forward, z + away, z - away)
+
+    def pass_on(distance):
+        for part in range(parts):
+            low, high = z - distance, z + distance
+
+            @pl.when(low >= 0)
+            def _():
+                row_copy(0, low, part, z, rows_ref).wait_recv()
+
+                @pl.when(z + 1 < line)
+                def _():
+                    row_copy(0, low, part, z + 1).start()
+
+            @pl.when(high < line)
+            def _():
+                row_copy(1, high, part, z, rows_ref).wait_recv()
+
+                @pl.when(z > 0)
+                def _():
+                    row_copy(1, high, part, z - 1).start()
+
+    def slot_names():
+        names = lax.broadcasted_iota(jnp.int32, (slots, tokens), 0) + z * slots
+        return names.astype(f32)
+
+    def select_copy(j, i):
+        q = lax.rem(p + i, plane)
+        return remote(
+            sel.at[j, q], xbuf.at[j, core, p], psend.at[j, i], precv.at[j, i], at(z, q)
+        )
+
+    def select(j):
+        block = block_of(j)
+        names = slot_names()
+        chosen = (names == meta[block, 0:1, :]) | (names == meta[block, 1:2, :])
+        place = jnp.where(chosen, 1.0, 0.0).astype(bf16)
+        source = rows_ref[...] if j == 0 else zbuf[block]
+        picked = jnp.dot(place, source, preferred_element_type=f32)
+        sel[j] = picked.reshape(plane, cap, width).astype(bf16)
+        for i in range(1, plane):
+            select_copy(j, i).start()
+        xbuf[j, core, p] = sel[j, p]
+
+    def partner_copy(j):
+        return remote(
+            xbuf.at[j, core], xbuf.at[j, core], tsend.at[j], trecv.at[j], partner
+        )
+
+    def collect(j):
+        for i in range(1, plane):
+            select_copy(j, i).wait_recv()
+        partner_copy(j).start()
+
+    def partial_copy(j):
+        return remote(ybuf.at[j, 1 - core], yin.at[j], ysend.at[j], yrecv.at[j], partner)
+
+    tall = 2 * slots
+    wide = 256
+
+    def multiply(j):
+        partner_copy(j).wait_recv()
+        if j == 0:
+            for copy in weights:
+                copy.wait()
+        if cap % 16 == 0:
+            batch = xbuf[j].reshape(tall, width)
+        else:
+            batch = xbuf[j].astype(f32).reshape(tall, width).astype(bf16)
+
+        @pl.loop(0, hidden.shape[1] // wide)
+        def _(tile):
+            columns = pl.ds(pl.multiple_of(tile * wide, wide), wide)
+            gate = jnp.dot(batch, gate_ref[:, columns], preferred_element_type=f32)
+            up = jnp.dot(batch, up_ref[:, columns], preferred_element_type=f32)
+            hidden[:, columns] = (gate * up / (1.0 + jnp.exp(-gate))).astype(bf16)
+
+        @pl.loop(0, width // wide)
+        def _(tile):
+            columns = pl.ds(pl.multiple_of(tile * wide, wide), wide)
+            value = jnp.dot(hidden[...], down_ref[:, columns], preferred_element_type=f32)
+            ybuf[j, :, :, :, columns] = value.reshape(2, plane, cap, wide).astype(bf16)
+
+        partial_copy(j).start()
+
+    def return_copy(j, i):
+        q = lax.rem(p + i, plane)
+        return remote(
+            sbuf.at[j, q], rbuf.at[j, p], rsend.at[j, i], rrecv.at[j, i], at(z, q)
+        )
+
+    def give_back(j):
+        partial_copy(j).wait_recv()
+        sbuf[j] = (ybuf[j, core].astype(f32) + yin[j].astype(f32)).astype(bf16)
+        for i in range(1, plane):
+            return_copy(j, i).start()
+        rbuf[j, p] = sbuf[j, p]
+
+    def chain_copy(way, block, part, target):
+        rows = pl.ds(part * chain_rows, chain_rows)
+        return remote(
+            csend.at[block, rows],
+            pin.at[way, block, rows],
+            ssend.at[block, part],
+            srecv.at[way, block, part],
+            at(target, p),
+        )
+
+    def combine(j):
+        for i in range(1, plane):
+            return_copy(j, i).wait_recv()
+        block = block_of(j)
+        names = slot_names()
+        weigh = jnp.where(names == meta[block, 0:1, :], meta[block, 2:3, :], 0.0)
+        weigh = weigh + jnp.where(names == meta[block, 1:2, :], meta[block, 3:4, :], 0.0)
+        weigh = weigh.T
+        high = weigh.astype(bf16)
+        low = (weigh - high.astype(f32)).astype(bf16)
+        if cap % 16 == 0:
+            back = rbuf[j].reshape(slots, width)
+        else:
+            back = rbuf[j].astype(f32).reshape(slots, width).astype(bf16)
+        total = jnp.dot(high, back, preferred_element_type=f32) + jnp.dot(
+            low, back, preferred_element_type=f32
+        )
+        if j == 0:
+            cbuf[block] = total + mixed_ref[...].astype(f32)
+        else:
+            cbuf[block] = total
+
+            @pl.when((z == 0) | (z == line - 1))
+            def _():
+                csend[block] = total.astype(bf16)
+
+            for part in range(chain):
+
+                @pl.when(z == 0)
+                def _():
+                    chain_copy(0, block, part, z + 1).start()
+
+                @pl.when(z == line - 1)
+                def _():
+                    chain_copy(1, block, part, z - 1).start()
+
+    select(0)
+    collect(0)
+    for i in range(1, line):
+        meta_copy(i).wait_recv()
+    for j in range(line):
+        if j + 1 < line:
+            pass_on(j + 1)
+            select(j + 1)
+        multiply(j)
+        if j + 1 < line:
+            collect(j + 1)
+        if j >= 1:
+            combine(j - 1)
+        give_back(j)
+    combine(line - 1)
+
+    def relay(way, block, last, step):
+        inside = (z < block) & (z > 0) if way == 0 else (z > block) & (z < line - 1)
+        fed = z > 0 if way == 0 else z < line - 1
+        for part in range(chain):
+            rows = pl.ds(part * chain_rows, chain_rows)
+
+            @pl.when(inside)
+            def _():
+                chain_copy(way, block, part, z).wait_recv()
+                total = cbuf[block, rows] + pin[way, block, rows].astype(f32)
+                csend[block, rows] = total.astype(bf16)
+                chain_copy(way, block, part, z + step).start()
+
+            @pl.when(fed & (z == block))
+            def _():
+                chain_copy(way, block, part, z).wait_recv()
+                cbuf[block, rows] = cbuf[block, rows] + pin[way, block, rows].astype(f32)
+
+    for i in range(1, line):
+        relay(0, i, line - 1, 1)
+        relay(1, line - 1 - i, 0, -1)
+    out_ref[...] = cbuf[z].astype(bf16)
+
+    for i in range(1, line):
+        meta_copy(i).wait_send()
+    for part in range(parts):
+        for block in range(line):
+
+            @pl.when((z >= block) & (z + 1 < line))
+            def _():
+                row_copy(0, block, part, z, rows_ref).wait_send()
+
+            @pl.when((z <= block) & (z > 0))
+            def _():
+                row_copy(1, block, part, z, rows_ref).wait_send()
+
+    for part in range(chain):
+        for block in range(line):
+
+            @pl.when(z != block)
+            def _():
+                chain_copy(0, block, part, z).wait_send()
+
+    for j in range(line):
+        for i in range(1, plane):
+            select_copy(j, i).wait_send()
+            return_copy(j, i).wait_send()
+        partner_copy(j).wait_send()
+        partial_copy(j).wait_send()
+
+
+def run_experts(rows, mixed, meta, gate, up, down, cap):
+    count = lax.axis_size("sp")
+    line = line_length(count)
+    plane = count // line
+    tokens, width = rows.shape
+    inner = gate.shape[2]
+    slots = plane * cap
+    parts, chain = 2, 4
+    bf16, f32 = jnp.bfloat16, jnp.float32
+    dma = pltpu.SemaphoreType.DMA
+    vmem = pl.BlockSpec(memory_space=pltpu.VMEM)
+    hbm = pl.BlockSpec(memory_space=pl.ANY)
+    return pl.pallas_call(
+        functools.partial(experts_kernel, line, plane, cap, parts, chain),
+        out_shape=jax.ShapeDtypeStruct((tokens, width), bf16),
+        in_specs=[vmem] * 3 + [hbm] * 3,
+        out_specs=vmem,
+        scratch_shapes=[
+            pltpu.VMEM((width, inner), bf16),
+            pltpu.VMEM((width, inner), bf16),
+            pltpu.VMEM((inner, width), bf16),
+            pltpu.VMEM((line, tokens, width), bf16),
+            pltpu.VMEM((line,) + meta.shape, f32),
+            pltpu.VMEM((line, plane, cap, width), bf16),
+            pltpu.VMEM((line, 2, plane, cap, width), bf16),
+            pltpu.VMEM((2 * slots, inner), bf16),
+            pltpu.VMEM((line, 2, plane, cap, width), bf16),
+            pltpu.VMEM((line, plane, cap, width), bf16),
+            pltpu.VMEM((line, plane, cap, width), bf16),
+            pltpu.VMEM((line, plane, cap, width), bf16),
+            pltpu.VMEM((line, tokens, width), f32),
+            pltpu.VMEM((line, tokens, width), bf16),
+            pltpu.VMEM((2, line, tokens, width), bf16),
+            dma((3, 4)),
+            dma((2, line, parts)),
+            dma((line, parts)),
+            dma((line,)),
+            dma((line,)),
+            dma((line, plane)),
+            dma((line, plane)),
+            dma((line,)),
+            dma((line,)),
+            dma((line,)),
+            dma((line,)),
+            dma((line, plane)),
+            dma((line, plane)),
+            dma((line, chain)),
+            dma((2, line, chain)),
+        ],
+        compiler_params=pltpu.CompilerParams(
+            collective_id=1, has_side_effects=True, vmem_limit_bytes=62 * 1024 * 1024
+        ),
+        name="experts",
+    )(rows, mixed, meta, gate, up, down)
 
 
 def shards(
@@ -129,10 +530,8 @@
         * lax.rsqrt(jnp.mean(mixed_float * mixed_float, axis=-1, keepdims=True) + 1e-06)
         * norm_gain
     ).astype(jnp.bfloat16)
-    d_model = residual.shape[1]
     experts = lax.axis_size("sp")
     capacity = 2 * tok_dev // experts
-    slots = experts * capacity
     top_count = expert_ids.shape[1]
     flat_routes = expert_ids.reshape(-1)
     onehot = (flat_routes[:, None] == jnp.arange(experts, dtype=jnp.int32)[None, :]).astype(
@@ -140,40 +539,17 @@
     )
     slot_rank = jnp.sum(jnp.cumsum(onehot, axis=0) * onehot, axis=1) - 1
     slot = (flat_routes * capacity + slot_rank).reshape(-1, top_count)
-    every_slot = jnp.arange(slots, dtype=jnp.int32)
-    place = jnp.zeros((slots, half), jnp.bool_)
-    weigh = jnp.zeros((half, slots), jnp.float32)
-    for choice in range(top_count):
-        column = slot[:, choice]
-        place = place | (every_slot[:, None] == column[None, :])
-        weigh = weigh + jnp.where(
-            column[:, None] == every_slot[None, :], expert_weights[:, choice][:, None], 0.0
-        )
-    outgoing = jnp.dot(
-        place.astype(jnp.bfloat16), normed_rows, preferred_element_type=jnp.float32
-    ).astype(jnp.bfloat16)
-    arrived = lax.all_to_all(
-        outgoing.reshape(experts, capacity, d_model), "sp", split_axis=0, concat_axis=0, tiled=True
-    ).reshape(slots, d_model)
-    both = jnp.concatenate([swap(arrived), arrived], axis=0)
-    hidden = expert_hidden(both, gate_experts[0], up_experts[0])
-    part = jnp.dot(hidden, down_experts[0], preferred_element_type=jnp.float32).astype(
-        jnp.bfloat16
-    )
-    got_part = swap(part[:slots])
-    part_here = part[slots:]
-    summed = (
-        part_here.astype(jnp.float32) + got_part.astype(jnp.float32)
-    ).astype(jnp.bfloat16)
-    returned = lax.all_to_all(
-        summed.reshape(experts, capacity, d_model), "sp", split_axis=0, concat_axis=0, tiled=True
-    ).reshape(slots, d_model)
-    weigh_high = weigh.astype(jnp.bfloat16)
-    weigh_low = (weigh - weigh_high.astype(jnp.float32)).astype(jnp.bfloat16)
-    expert_sum = jnp.dot(weigh_high, returned, preferred_element_type=jnp.float32) + jnp.dot(
-        weigh_low, returned, preferred_element_type=jnp.float32
-    )
-    return (mixed_float + expert_sum).astype(jnp.bfloat16)
+    meta = jnp.concatenate(
+        [
+            slot.T.astype(jnp.float32),
+            expert_weights.T,
+            jnp.zeros((8 - 2 * top_count, half), jnp.float32),
+        ],
+        axis=0,
+    )
+    return run_experts(
+        normed_rows, mixed_rows, meta, gate_experts, up_experts, down_experts, capacity
+    )
 
 
 def solution(mesh):

time: 206 us -> 175 us (0.85)
  the two profiles are of different devices: /device:TPU:14 before, /device:TPU:0 now
where the time goes in v1:
time: 175 us
  Pallas kernels  130 us (74%)
  starting transfers between devices  20.7 us (12%)
  local copies, waits for them, and re-layouts  6.4 us (4%)
  other arithmetic  5.98 us (3%)
  waiting for transfers between devices  5.81 us (3%)
  matrix products  5.25 us (3%)
    pallas_call x1, Pallas kernels, run_experts(): pl.pallas_call(functools.partial(experts_kernel, line, plane, cap, parts,...  130 us
    ppermute x4, starting transfers between devices, shift(): lax.ppermute(packed, 'sp', [(i, i + distance) for i in range(count - dist...  20.7 us
    ppermute x4, waiting for transfers between devices, shift(): lax.ppermute(packed, 'sp', [(i, i + distance) for i in range(count - dist...  4.76 us
    unnamed x19, local copies, waits for them, and re-layouts  4.34 us
  transfers between devices with their start and end apart: 5, of which 4 were waited for; matrix products, arithmetic and copies ran while one was open for 3% of the time, Pallas kernels for 0%

profile of v1, /device:TPU:0, one launch (start us, length us, event | category | flops | bytes accessed | tf_op | source)
XLA Modules:
  0.0 174.5 jit_solution(18038624354741444232)
XLA Ops:
  0.0 1.3 reduce-window.14
  1.8 1.1 copy.36
  3.0 1.1 copy.37
  4.3 0.2 multiply_cosine_fusion
  4.7 0.3 convolution_bitcast_fusion.1
  5.4 4.9 %collective-permute-start = (bf16[66,512]{1,0:T(8,128)(2,1)S(1)}, bf16[66,512]{1,0:T(8,128)(2,1)S(1)}, u32[]{:S(2)}, u32[]{:S(2)}) collective-permute-start(bf16[66,512]{1,0:T(8,128)(2,1)S(1)} %pad_maximum_fusion.6), channel_id=1, source_target_pairs={{0,2},{2,4},{4,6},{6,8},{8,10},{10,12},{12,14},{14,16},{16,18},{18... | collective-permute-start | bytes 202760 | tf_op jit(solution)/shard_map/ppermute | solution.py:34
  10.4 1.0 fusion.24
  11.5 1.2 fusion.7
  13.2 4.4 %collective-permute-start.1 = (bf16[66,512]{1,0:T(8,128)(2,1)S(1)}, bf16[66,512]{1,0:T(8,128)(2,1)S(1)}, u32[]{:S(2)}, u32[]{:S(2)}) collective-permute-start(bf16[66,512]{1,0:T(8,128)(2,1)S(1)} %pad_maximum_fusion.7), channel_id=1, source_target_pairs={{0,4},{2,6},{4,8},{6,10},{8,12},{10,14},{12,16},{14,18},{16,20},{1... | collective-permute-start | bytes 202760 | tf_op jit(solution)/shard_map/ppermute | solution.py:34
  17.8 0.6 reduce-window.16
  18.4 1.2 collective-permute-done.1
  19.7 6.1 %collective-permute-start.2 = (bf16[66,512]{1,0:T(8,128)(2,1)S(1)}, bf16[66,512]{1,0:T(8,128)(2,1)S(1)}, u32[]{:S(2)}, u32[]{:S(2)}) collective-permute-start(bf16[66,512]{1,0:T(8,128)(2,1)S(1)} %pad_maximum_fusion.8), channel_id=1, source_target_pairs={{0,8},{2,10},{4,12},{6,14},{8,16},{10,18},{12,20},{14,22},{16,24},... | collective-permute-start | bytes 202760 | tf_op jit(solution)/shard_map/ppermute | solution.py:34
  26.0 1.7 collective-permute-done.2
  27.9 5.3 %collective-permute-start.3 = (bf16[66,512]{1,0:T(8,128)(2,1)S(1)}, bf16[66,512]{1,0:T(8,128)(2,1)S(1)}, u32[]{:S(2)}, u32[]{:S(2)}) collective-permute-start(bf16[66,512]{1,0:T(8,128)(2,1)S(1)} %pad_maximum_fusion.9), channel_id=1, source_target_pairs={{0,16},{2,18},{4,20},{6,22},{8,24},{10,26},{12,28},{14,30},{1,17},... | collective-permute-start | bytes 202760 | tf_op jit(solution)/shard_map/ppermute | solution.py:34
  33.2 1.9 %collective-permute-done.3 = bf16[66,512]{1,0:T(8,128)(2,1)S(1)} collective-permute-done((bf16[66,512]{1,0:T(8,128)(2,1)S(1)}, bf16[66,512]{1,0:T(8,128)(2,1)S(1)}, u32[]{:S(2)}, u32[]{:S(2)}) %collective-permute-start.3) | collective-permute-done | bytes 67616 | tf_op jit(solution)/shard_map/ppermute | solution.py:34
  35.3 0.4 multiply_reduce_fusion
  36.1 1.1 fusion.26
  37.2 0.4 convolution_convert_fusion
  38.1 0.7 maximum_maximum_fusion.meta_ref
  38.8 1.0 collective-permute-done.4
  39.8 1.9 %fusion.11 = (f32[128]{0:T(128)S(1)}, bf16[128,2048]{1,0:T(8,128)(2,1)S(1)}) fusion(bf16[128,2048]{1,0:T(8,128)(2,1)} %collective-permute-done.4, bf16[512,2048]{1,0:T(8,128)(2,1)S(1)} %copy-done, bf16[256,512]{1,0:T(8,128)(2,1)S(1)} %fusion.26, s32[]{:T(128)S(6)} %select_n.15, bf16[128,2048]{1,0:T(8,128)(2,1)} %param.21), kind=kOutput, calls=%fused_computation.15 | convolution fusion | flops 271056768 | bytes 3801604 | tf_op jit(solution)/shard_map/dot_general | solution.py:524
  41.7 1.0 fusion.13.rows_ref
  42.7 129.9 %experts.1 = bf16[128,2048]{1,0:T(8,128)(2,1)} custom-call(bf16[128,2048]{1,0:T(8,128)(2,1)} %fusion.13.rows_ref, bf16[128,2048]{1,0:T(8,128)(2,1)} %copy-done.1, f32[8,128]{1,0:T(8,128)} %maximum_maximum_fusion.meta_ref, bf16[1,2048,1792]{2,1,0:T(8,128)(2,1)} %gate_hbm.1, bf16[1,2048,1792]{2,1,0:T(8,128)(2,1)} %up_hbm.1, bf16[1,1792,2048]{2,1,0:T(8,128)(2,1)} %down_hbm.1), custom_call_target="tpu_custom_call" | custom-call | tf_op jit(solution)/shard_map/experts/pallas_call | solution.py:415
  172.7 1.9 %copy.50 = bf16[128,2048]{1,0:T(8,128)(2,1)} copy(bf16[128,2048]{1,0:T(8,128)(2,1)} %experts.1) | data formatting | bytes 1048576
  (76 shorter events, 3.6 us)
Async XLA Ops:
  0.0 4.1 %copy-start.2 = (bf16[256,512]{1,0:T(8,128)(2,1)S(1)}, bf16[256,512]{1,0:T(8,128)(2,1)}, u32[]{:S(2)}) copy-start(bf16[256,512]{1,0:T(8,128)(2,1)} %param.16) | copy-start | bytes 786436
  5.4 7.7 %collective-permute-start = (bf16[66,512]{1,0:T(8,128)(2,1)S(1)}, bf16[66,512]{1,0:T(8,128)(2,1)S(1)}, u32[]{:S(2)}, u32[]{:S(2)}) collective-permute-start(bf16[66,512]{1,0:T(8,128)(2,1)S(1)} %pad_maximum_fusion.6), channel_id=1, source_target_pairs={{0,2},{2,4},{4,6},{6,8},{8,10},{10,12},{12,14},{14,16},{16,18},{18... | collective-permute-start | bytes 202760 | tf_op jit(solution)/shard_map/ppermute | solution.py:34
  11.5 1.4 copy-start.4
  11.5 6.3 %copy-start.5 = (f32[512]{0:T(512)S(1)}, f32[512]{0:T(512)}, u32[]{:S(2)}) copy-start(f32[512]{0:T(512)} %param.19) | copy-start | bytes 6148
  13.2 6.3 %collective-permute-start.1 = (bf16[66,512]{1,0:T(8,128)(2,1)S(1)}, bf16[66,512]{1,0:T(8,128)(2,1)S(1)}, u32[]{:S(2)}, u32[]{:S(2)}) collective-permute-start(bf16[66,512]{1,0:T(8,128)(2,1)S(1)} %pad_maximum_fusion.7), channel_id=1, source_target_pairs={{0,4},{2,6},{4,8},{6,10},{8,12},{10,14},{12,16},{14,18},{16,20},{1... | collective-permute-start | bytes 202760 | tf_op jit(solution)/shard_map/ppermute | solution.py:34
  19.7 8.1 %collective-permute-start.2 = (bf16[66,512]{1,0:T(8,128)(2,1)S(1)}, bf16[66,512]{1,0:T(8,128)(2,1)S(1)}, u32[]{:S(2)}, u32[]{:S(2)}) collective-permute-start(bf16[66,512]{1,0:T(8,128)(2,1)S(1)} %pad_maximum_fusion.8), channel_id=1, source_target_pairs={{0,8},{2,10},{4,12},{6,14},{8,16},{10,18},{12,20},{14,22},{16,24},... | collective-permute-start | bytes 202760 | tf_op jit(solution)/shard_map/ppermute | solution.py:34
  27.9 7.3 %collective-permute-start.3 = (bf16[66,512]{1,0:T(8,128)(2,1)S(1)}, bf16[66,512]{1,0:T(8,128)(2,1)S(1)}, u32[]{:S(2)}, u32[]{:S(2)}) collective-permute-start(bf16[66,512]{1,0:T(8,128)(2,1)S(1)} %pad_maximum_fusion.9), channel_id=1, source_target_pairs={{0,16},{2,18},{4,20},{6,22},{8,24},{10,26},{12,28},{14,30},{1,17},... | collective-permute-start | bytes 202760 | tf_op jit(solution)/shard_map/ppermute | solution.py:34
  35.3 1.9 %copy-start = (bf16[512,2048]{1,0:T(8,128)(2,1)S(1)}, bf16[512,2048]{1,0:T(8,128)(2,1)}, u32[]{:S(2)}) copy-start(bf16[512,2048]{1,0:T(8,128)(2,1)} %param.20) | copy-start | bytes 6291460
  36.1 2.0 %copy-start.6 = (f32[128,2]{0,1:T(2,128)S(1)}, f32[128,2]{0,1:T(2,128)}, u32[]{:S(2)}) copy-start(f32[128,2]{0,1:T(2,128)} %param.24) | copy-start | bytes 3076
  37.7 4.0 %copy-start.3 = (f32[2048]{0:T(1024)S(1)}, f32[2048]{0:T(1024)}, u32[]{:S(2)}) copy-start(f32[2048]{0:T(1024)} %param.22) | copy-start | bytes 24580
  37.7 2.1 %collective-permute-start.4 = (bf16[128,2048]{1,0:T(8,128)(2,1)S(1)}, bf16[128,2048]{1,0:T(8,128)(2,1)}, u32[]{:S(2)}, u32[]{:S(2)}) collective-permute-start(bf16[128,2048]{1,0:T(8,128)(2,1)S(1)} %convolution_convert_fusion), channel_id=1, source_target_pairs={{0,1},{1,0},{2,3},{3,2},{4,5},{5,4},{6,7},{7,6},{8,9},{9,8},{10,11... | collective-permute-start | bytes 1572872 | tf_op jit(solution)/shard_map/ppermute | solution.py:21
  41.7 1.0 copy-start.1

commit v2 on v1

v2 whole, which is shorter than its diff:
```python
import functools

import jax
import jax.numpy as jnp
from jax import lax
from jax.experimental import pallas as pl
from jax.experimental.pallas import tpu as pltpu
from jax.sharding import PartitionSpec as P

MESH = pl.DeviceIdType.MESH


def line_length(count):
    size = 1
    while size * size * size < count:
        size *= 2
    return size


def layer_kernel(
    line,
    plane,
    cap,
    parts,
    halves,
    chain,
    query_hbm,
    key_hbm,
    value_hbm,
    gates_hbm,
    decay_ref,
    gain_ref,
    project_hbm,
    residual_hbm,
    norm_ref,
    route_ref,
    cos_ref,
    sin_ref,
    gate_hbm,
    up_hbm,
    down_hbm,
    out_ref,
    query_ref,
    key_ref,
    value_ref,
    gates_ref,
    project_ref,
    residual_ref,
    running_ref,
    by_head_ref,
    turned_query,
    turned_key,
    start_query,
    within_ref,
    normed_ref,
    away_ref,
    got_ref,
    mixed_ref,
    meta_ref,
    state_out,
    state_in,
    totals,
    before_ref,
    plane_state,
    plane_total,
    line_state,
    line_total,
    carry_ref,
    back_state,
    start_state,
    lsem,
    asend,
    arecv,
    bsend,
    brecv,
    ctsend,
    ctrecv,
    dsend,
    drecv,
    esend,
    erecv,
    gate_ref,
    up_ref,
    down_ref,
    zbuf,
    meta,
    sel,
    xbuf,
    hidden,
    ybuf,
    yin,
    sbuf,
    rbuf,
    cbuf,
    csend,
    pin,
    wsem,
    zsend,
    zrecv,
    msend,
    mrecv,
    psend,
    precv,
    tsend,
    trecv,
    ysend,
    yrecv,
    rsend,
    rrecv,
    ssend,
    srecv,
):
    sp, core = lax.axis_index("sp"), lax.axis_index("tp")
    z, p = sp // plane, lax.rem(sp, plane)
    length, channels = query_ref.shape
    tokens, width = residual_ref.shape
    lanes = cos_ref.shape[1]
    heads = decay_ref.shape[1]
    size = channels // heads
    pack = lanes // size
    groups = channels // lanes
    slice_rows = state_out.shape[1]
    slots = plane * cap
    f32, bf16 = jnp.float32, jnp.bfloat16

    def at(line_place, plane_place):
        return {"sp": line_place * plane + plane_place, "tp": core}

    partner = {"sp": sp, "tp": 1 - core}

    def remote(src, dst, send, recv, device):
        return pltpu.make_async_remote_copy(
            src_ref=src,
            dst_ref=dst,
            send_sem=send,
            recv_sem=recv,
            device_id=device,
            device_id_type=MESH,
        )

    loads = [
        pltpu.make_async_copy(source, target, lsem.at[number])
        for number, (source, target) in enumerate(
            (
                (query_hbm, query_ref),
                (key_hbm, key_ref),
                (value_hbm, value_ref),
                (gates_hbm, gates_ref),
                (project_hbm, project_ref),
                (residual_hbm, residual_ref),
            )
        )
    ]
    for copy in loads:
        copy.start()

    weights = []
    for number, (source, target) in enumerate(
        ((gate_hbm, gate_ref), (up_hbm, up_ref), (down_hbm, down_ref))
    ):
        depth = target.shape[0] // 4
        for piece in range(4):
            part = pl.ds(piece * depth, depth)
            weights.append(
                pltpu.make_async_copy(
                    source.at[0, part], target.at[part], wsem.at[number, piece]
                )
            )

    barrier = pltpu.get_barrier_semaphore()
    peers = [at(lax.rem(z + i, line), p) for i in range(1, line)]
    peers += [at(z, lax.rem(p + i, plane)) for i in range(1, plane)] + [partner]
    for peer in peers:
        pl.semaphore_signal(barrier, inc=1, device_id=peer, device_id_type=MESH)
    for copy in weights:
        copy.start()

    lane = lax.broadcasted_iota(jnp.int32, (1, lanes), 1)
    contract = (((1,), (1,)), ((), ()))
    upright = (((0,), (0,)), ((), ()))

    def place_of(group):
        return pl.ds(pl.multiple_of(group * lanes, lanes), lanes)

    def by_lane(pieces):
        value = pieces[-1]
        for number in range(pack - 2, -1, -1):
            value = jnp.where(lane < (number + 1) * size, pieces[number], value)
        return value

    count = line * plane
    expert = lax.broadcasted_iota(jnp.int32, (count, tokens), 0).astype(f32)
    first_hot = jnp.where(expert == route_ref[0:1, :], 1.0, 0.0)
    second_hot = jnp.where(expert == route_ref[1:2, :], 1.0, 0.0)
    earlier = lax.broadcasted_iota(jnp.int32, (tokens, tokens), 0) < (
        lax.broadcasted_iota(jnp.int32, (tokens, tokens), 1)
    )
    taken = jnp.dot(
        (first_hot + second_hot).astype(bf16),
        jnp.where(earlier, 1.0, 0.0).astype(bf16),
        preferred_element_type=f32,
    )
    first_rank = jnp.sum(first_hot * taken, axis=0, keepdims=True)
    second_rank = jnp.sum(second_hot * taken, axis=0, keepdims=True)
    meta_ref[...] = route_ref[...]
    meta_ref[0:1, :] = route_ref[0:1, :] * cap + first_rank
    meta_ref[1:2, :] = route_ref[1:2, :] * cap + second_rank

    rows_of = lax.broadcasted_iota(jnp.int32, (length, length), 0)
    columns_of = lax.broadcasted_iota(jnp.int32, (length, length), 1)
    causal = rows_of >= columns_of
    lower = jnp.where(causal, 1.0, 0.0).astype(bf16)
    upper = jnp.where(rows_of <= columns_of, 1.0, 0.0).astype(bf16)
    spread = lax.broadcasted_iota(jnp.int32, (heads, channels), 1) // size == (
        lax.broadcasted_iota(jnp.int32, (heads, channels), 0)
    )
    spread = jnp.where(spread, 1.0, 0.0).astype(bf16)
    rest = decay_ref[...]
    running, by_head = 0.0, 0.0
    for _ in range(3):
        piece = rest.astype(bf16)
        rest = rest - piece.astype(f32)
        wide_piece = jnp.dot(piece, spread, preferred_element_type=f32).astype(bf16)
        running = running + jnp.dot(lower, wide_piece, preferred_element_type=f32)
        by_head = by_head + lax.dot_general(piece, upper, upright, preferred_element_type=f32)
    running_ref[...] = running
    by_head_ref[...] = by_head

    swapped = lax.broadcasted_iota(jnp.int32, (lanes, lanes), 0) == (
        lax.broadcasted_iota(jnp.int32, (lanes, lanes), 1) ^ (size // 2)
    )
    swapped = jnp.where(swapped, 1.0, 0.0).astype(bf16)
    for copy in loads[:3]:
        copy.wait()

    def turn(block):
        other = jnp.dot(block, swapped, preferred_element_type=f32)
        return block.astype(f32) * cos_ref[...] + other * sin_ref[...]

    for group in range(groups):
        where = pl.ds(group * lanes, lanes)
        run = running_ref[:, where]
        query = turn(query_ref[:, where])
        key = turn(key_ref[:, where]) * size ** (-0.5)
        turned_query[:, where] = query.astype(bf16)
        turned_key[:, where] = key.astype(bf16)
        start_query[:, where] = (query * jnp.exp(run)).astype(bf16)
        end = run[length - 1 : length, :]
        final = lax.dot_general(
            (key * jnp.exp(end - run)).astype(bf16),
            value_ref[:, where],
            upright,
            preferred_element_type=f32,
        )
        state = by_lane([final[n * size : (n + 1) * size, :] for n in range(pack)])
        totals[p, group] = jnp.broadcast_to(end, totals.shape[2:])
        per = size // slice_rows if slice_rows < size else 1
        deep = min(slice_rows, size)
        for part in range(per):
            row = group * size + part * deep
            state_out[row // slice_rows, pl.ds(row % slice_rows, deep), :] = state[
                part * deep : (part + 1) * deep, :
            ].astype(bf16)
    state_in[p] = state_out[p]

    pl.semaphore_wait(barrier, len(peers))

    def state_copy(i):
        q = lax.rem(p + i, plane)
        return remote(
            state_out.at[q], state_in.at[p], asend.at[i], arecv.at[i], at(z, q)
        )

    def total_copy(i):
        q = lax.rem(p + i, plane)
        return remote(totals.at[p], totals.at[p], bsend.at[i], brecv.at[i], at(z, q))

    for i in range(1, plane):
        state_copy(i).start()
        total_copy(i).start()

    def meta_copy(i):
        return remote(
            meta_ref, meta.at[z], msend.at[i], mrecv.at[i], at(lax.rem(z + i, line), p)
        )

    for i in range(1, line):
        meta_copy(i).start()

    def attend(lo, hi):
        @pl.loop(lo, hi)
        def _(group):
            where = place_of(group)
            query, key, value = turned_query[:, where], turned_key[:, where], value_ref[:, where]
            run = running_ref[:, where]
            total = []
            for number in range(pack):
                mine = (lane >= number * size) & (lane < (number + 1) * size)
                masked = jnp.where(mine, query, jnp.zeros_like(query))
                score = lax.dot_general(masked, key, contract, preferred_element_type=f32)
                gap = run[:, number * size : number * size + 1] - by_head_ref[
                    pl.ds(group * pack + number, 1), :
                ]
                ok = lax.broadcasted_iota(jnp.int32, (length, length), 0) >= (
                    lax.broadcasted_iota(jnp.int32, (length, length), 1)
                )
                weight = jnp.where(ok, jnp.exp(jnp.where(ok, gap, 0.0)), 0.0)
                total.append(
                    jnp.dot((score * weight).astype(bf16), value, preferred_element_type=f32)
                )
            within_ref[:, where] = by_lane(total)

    attend(0, groups // 2)

    mine = p * slice_rows // size
    for i in range(1, plane):
        state_copy(i).wait_recv()
        total_copy(i).wait_recv()
    held = jnp.zeros((slice_rows, lanes), f32)
    elapsed = jnp.zeros((1, lanes), f32)
    for q in range(plane):
        before_ref[q] = held
        step = totals[q, mine][0:1, :]
        held = jnp.exp(step) * held + state_in[q].astype(f32)
        elapsed = elapsed + step
    plane_state[...] = held.astype(bf16)
    plane_total[...] = jnp.broadcast_to(elapsed, plane_total.shape)

    def line_state_copy(i):
        return remote(
            plane_state, line_state.at[z], ctsend.at[i, 0], ctrecv.at[i, 0], at(z + i, p)
        )

    def line_total_copy(i):
        return remote(
            plane_total, line_total.at[z], ctsend.at[i, 1], ctrecv.at[i, 1], at(z + i, p)
        )

    for i in range(1, line):

        @pl.when(z + i < line)
        def _():
            line_state_copy(i).start()
            line_total_copy(i).start()

    attend(groups // 2, groups)

    carry_ref[...] = jnp.zeros_like(carry_ref)
    for i in range(line - 1, 0, -1):

        @pl.when(z >= i)
        def _():
            line_state_copy(i).wait_recv()
            line_total_copy(i).wait_recv()
            step = line_total[z - i][0:1, :]
            carry_ref[...] = jnp.exp(step) * carry_ref[...] + line_state[z - i].astype(f32)

    elapsed = jnp.zeros((1, lanes), f32)
    for q in range(plane):
        value = before_ref[q] + jnp.exp(elapsed) * carry_ref[...]
        back_state[q] = value.astype(bf16)
        elapsed = elapsed + totals[q, mine][0:1, :]

    def start_copy(i):
        q = lax.rem(p + i, plane)
        return remote(
            back_state.at[q], start_state.at[p], dsend.at[i], drecv.at[i], at(z, q)
        )

    for i in range(1, plane):
        start_copy(i).start()
    start_state[p] = back_state[p]
    for copy in loads[3:]:
        copy.wait()
    for i in range(1, plane):
        start_copy(i).wait_recv()

    for group in range(groups):
        where = pl.ds(group * lanes, lanes)
        pieces = []
        for part in range(max(1, size // slice_rows)):
            row = group * size + part * slice_rows
            deep = min(slice_rows, size)
            pieces.append(start_state[row // slice_rows, pl.ds(row % slice_rows, deep), :])
        state = pieces[0] if len(pieces) == 1 else jnp.concatenate(pieces, axis=0)
        diagonal = jnp.concatenate(
            [
                jnp.where(
                    (lane >= n * size) & (lane < (n + 1) * size), state, jnp.zeros_like(state)
                )
                for n in range(pack)
            ],
            axis=0,
        )
        retained = within_ref[:, where] + jnp.dot(
            start_query[:, where], diagonal, preferred_element_type=f32
        )
        square = retained * retained
        sums = [
            jnp.sum(
                jnp.where((lane >= n * size) & (lane < (n + 1) * size), square, 0.0),
                axis=1,
                keepdims=True,
            )
            for n in range(pack)
        ]
        mean = by_lane(sums) * (1.0 / size)
        gates = gates_ref[:, where].astype(f32)
        normed = retained * lax.rsqrt(mean + 1e-06) * gain_ref[:, where]
        normed = normed * (gates / (1.0 + jnp.exp(-gates)))
        normed_ref[:, where] = normed.astype(bf16)

    def away_copy(h):
        columns = pl.ds(h * (width // 2), width // 2)
        return remote(
            away_ref.at[:, columns], got_ref.at[:, columns], esend.at[h], erecv.at[h], partner
        )

    away_rows = pl.ds(pl.multiple_of((1 - core) * tokens, tokens), tokens)
    here_rows = pl.ds(pl.multiple_of(core * tokens, tokens), tokens)
    for h in range(2):
        columns = pl.ds(h * (width // 2), width // 2)
        away_ref[:, columns] = jnp.dot(
            normed_ref[away_rows, :], project_ref[:, columns], preferred_element_type=f32
        ).astype(bf16)
        away_copy(h).start()
    squares = jnp.zeros((tokens, 1), f32)
    for h in range(2):
        columns = pl.ds(h * (width // 2), width // 2)
        here = jnp.dot(
            normed_ref[here_rows, :], project_ref[:, columns], preferred_element_type=f32
        ).astype(bf16)
        away_copy(h).wait_recv()
        projected = here.astype(f32) + got_ref[:, columns].astype(f32)
        mixed = (residual_ref[:, columns].astype(f32) + projected).astype(bf16)
        mixed_ref[:, columns] = mixed
        mixed = mixed.astype(f32)
        squares = squares + jnp.sum(mixed * mixed, axis=1, keepdims=True)
    scale = lax.rsqrt(squares * (1.0 / width) + 1e-06)
    for h in range(2):
        columns = pl.ds(h * (width // 2), width // 2)
        normed = mixed_ref[:, columns].astype(f32) * scale * norm_ref[:, columns]
        zbuf[z, :, columns] = normed.astype(bf16)

    piece_rows = tokens // parts
    chain_width = width // chain

    def row_copy(way, block, part, target):
        rows = pl.ds(part * piece_rows, piece_rows)
        return remote(
            zbuf.at[block, rows],
            zbuf.at[block, rows],
            zsend.at[way, block, part],
            zrecv.at[block, part],
            at(target, p),
        )

    for part in range(parts):

        @pl.when(z + 1 < line)
        def _():
            row_copy(0, z, part, z + 1).start()

        @pl.when(z > 0)
        def _():
            row_copy(1, z, part, z - 1).start()

    meta[z] = meta_ref[...]

    near = jnp.minimum(z, line - 1 - z)
    longer_up = z < line - 1 - z

    def block_of(place):
        both = place <= 2 * near
        away = jnp.where(both, (place + 1) // 2, place - near)
        forward = jnp.where(both, place % 2 == 1, longer_up)
        return jnp.where(forward, z + away, z - away)

    def pass_on(distance, lo, hi):
        for part in range(lo, hi):
            low, high = z - distance, z + distance

            @pl.when(low >= 0)
            def _():
                row_copy(0, low, part, z).wait_recv()

                @pl.when(z + 1 < line)
                def _():
                    row_copy(0, low, part, z + 1).start()

            @pl.when(high < line)
            def _():
                row_copy(1, high, part, z).wait_recv()

                @pl.when(z > 0)
                def _():
                    row_copy(1, high, part, z - 1).start()

    def slot_names():
        names = lax.broadcasted_iota(jnp.int32, (slots, tokens), 0) + z * slots
        return names.astype(f32)

    def select_copy(j, i):
        q = lax.rem(p + i, plane)
        return remote(
            sel.at[j, q], xbuf.at[j, core, p], psend.at[j, i], precv.at[j, i], at(z, q)
        )

    def select(j):
        block = block_of(j)
        names = slot_names()
        chosen = (names == meta[block, 0:1, :]) | (names == meta[block, 1:2, :])
        place = jnp.where(chosen, 1.0, 0.0).astype(bf16)
        picked = jnp.dot(place, zbuf[block], preferred_element_type=f32)
        sel[j] = picked.reshape(plane, cap, width).astype(bf16)
        for i in range(1, plane):
            select_copy(j, i).start()
        xbuf[j, core, p] = sel[j, p]

    def partner_copy(j):
        return remote(
            xbuf.at[j, core], xbuf.at[j, core], tsend.at[j], trecv.at[j], partner
        )

    def collect(j):
        for i in range(1, plane):
            select_copy(j, i).wait_recv()
        partner_copy(j).start()

    half = width // halves

    def partial_copy(j, h):
        columns = pl.ds(h * half, half)
        return remote(
            ybuf.at[j, 1 - core, :, :, columns],
            yin.at[j, :, :, columns],
            ysend.at[j, h],
            yrecv.at[j, h],
            partner,
        )

    tall = 2 * slots
    wide = 256

    def widen(j, lo, hi):
        if lo == hi:
            return
        if cap % 16 == 0:
            batch = xbuf[j].reshape(tall, width)
        else:
            batch = xbuf[j].astype(f32).reshape(tall, width).astype(bf16)

        @pl.loop(lo, hi)
        def _(tile):
            columns = pl.ds(pl.multiple_of(tile * wide, wide), wide)
            gate = jnp.dot(batch, gate_ref[:, columns], preferred_element_type=f32)
            up = jnp.dot(batch, up_ref[:, columns], preferred_element_type=f32)
            hidden[:, columns] = (gate * up / (1.0 + jnp.exp(-gate))).astype(bf16)

    def narrow(j, h):
        @pl.loop(h * (half // wide), (h + 1) * (half // wide))
        def _(tile):
            columns = pl.ds(pl.multiple_of(tile * wide, wide), wide)
            value = jnp.dot(hidden[...], down_ref[:, columns], preferred_element_type=f32)
            ybuf[j, :, :, :, columns] = value.reshape(2, plane, cap, wide).astype(bf16)

        partial_copy(j, h).start()

    def return_copy(j, i, h):
        q = lax.rem(p + i, plane)
        columns = pl.ds(h * half, half)
        return remote(
            sbuf.at[j, q, :, columns],
            rbuf.at[j, p, :, columns],
            rsend.at[j, i, h],
            rrecv.at[j, i, h],
            at(z, q),
        )

    def give_back(j, h):
        columns = pl.ds(h * half, half)
        partial_copy(j, h).wait_recv()
        total = ybuf[j, core, :, :, columns].astype(f32) + yin[j, :, :, columns].astype(f32)
        sbuf[j, :, :, columns] = total.astype(bf16)
        for i in range(1, plane):
            return_copy(j, i, h).start()
        rbuf[j, p, :, columns] = sbuf[j, p, :, columns]

    def chain_copy(way, block, part, target):
        columns = pl.ds(part * chain_width, chain_width)
        return remote(
            csend.at[block, :, columns],
            pin.at[way, block, :, columns],
            ssend.at[block, part],
            srecv.at[way, block, part],
            at(target, p),
        )

    def weigh_of(j):
        block = block_of(j)
        names = slot_names()
        weigh = jnp.where(names == meta[block, 0:1, :], meta[block, 2:3, :], 0.0)
        weigh = weigh + jnp.where(names == meta[block, 1:2, :], meta[block, 3:4, :], 0.0)
        weigh = weigh.T
        high = weigh.astype(bf16)
        return high, (weigh - high.astype(f32)).astype(bf16)

    def combine(j, h, weigh):
        for i in range(1, plane):
            return_copy(j, i, h).wait_recv()
        block = block_of(j)
        high, low = weigh
        columns = pl.ds(h * half, half)
        if cap % 16 == 0:
            back = rbuf[j, :, :, columns].reshape(slots, half)
        else:
            back = rbuf[j, :, :, columns].astype(f32).reshape(slots, half).astype(bf16)
        total = jnp.dot(high, back, preferred_element_type=f32) + jnp.dot(
            low, back, preferred_element_type=f32
        )
        if j == 0:
            cbuf[block, :, columns] = total + mixed_ref[:, columns].astype(f32)
        else:
            cbuf[block, :, columns] = total

            @pl.when((z == 0) | (z == line - 1))
            def _():
                csend[block, :, columns] = total.astype(bf16)

            for part in range(h * chain // halves, (h + 1) * chain // halves):

                @pl.when(z == 0)
                def _():
                    chain_copy(0, block, part, z + 1).start()

                @pl.when(z == line - 1)
                def _():
                    chain_copy(1, block, part, z - 1).start()

    def relay(way, block, part):
        before = jnp.where(way == 0, z < block, z > block)
        inside = before & (z > 0) & (z < line - 1)
        columns = pl.ds(part * chain_width, chain_width)

        @pl.when(inside)
        def _():
            chain_copy(way, block, part, z).wait_recv()
            total = cbuf[block, :, columns] + pin[way, block, :, columns].astype(f32)
            csend[block, :, columns] = total.astype(bf16)
            chain_copy(way, block, part, z + 1 - 2 * way).start()

    first_way = jnp.where(2 * z < line, 0, 1)

    def relays(i, lo, hi):
        def one(way, part):
            relay(way, jnp.where(way == 0, i, line - 1 - i), part)

        for part in range(lo, hi + lag):
            if part < hi:
                one(first_way, part)
            if part >= lo + lag:
                one(1 - first_way, part - lag)

    lag = chain // 2
    tiles = hidden.shape[1] // wide
    sc = jax.named_scope
    with sc("select#0"):
        select(0)
    with sc("meta"):
        for i in range(1, line):
            meta_copy(i).wait_recv()
    with sc("pass#1a"):
        pass_on(1, 0, parts // 2)
    with sc("collect#0"):
        collect(0)
    for j in range(line):
        last = j + 1 == line
        cut = max(0, tiles - j * tiles // 2)
        with sc(f"xwait#{j}"):
            partner_copy(j).wait_recv()
            if j == 0:
                for copy in weights:
                    copy.wait()
        with sc(f"widen#{j}a"):
            widen(j, 0, cut)
        if not last:
            with sc(f"pass#{j + 1}b"):
                pass_on(j + 1, parts // 2, parts)
            with sc(f"select#{j + 1}"):
                select(j + 1)
        with sc(f"widen#{j}b"):
            widen(j, cut, tiles)
        if j >= 1:
            with sc(f"combine#{j - 1}"):
                weigh = weigh_of(j - 1)
                for h in range(halves):
                    combine(j - 1, h, weigh)
        with sc(f"narrow#{j}a"):
            narrow(j, 0)
        with sc(f"narrow#{j}b"):
            for h in range(1, halves):
                narrow(j, h)
        if j + 2 < line:
            with sc(f"pass#{j + 2}a"):
                pass_on(j + 2, 0, parts // 2)
        if not last:
            with sc(f"collect#{j + 1}"):
                collect(j + 1)
        with sc(f"give#{j}"):
            for h in range(halves):
                give_back(j, h)
        if 2 <= j < line - 2:
            relays(j, 0, chain)
    weigh = weigh_of(line - 1)
    share = chain // halves
    for h in range(halves):
        if line > 2:
            with sc(f"relays#a{h}"):
                relays(line - 2, h * share, h * share + share // 2)
        with sc(f"combine#last{h}"):
            combine(line - 1, h, weigh)
        if line > 2:
            with sc(f"relays#b{h}"):
                relays(line - 2, h * share + share // 2, (h + 1) * share)
    with sc("relays#c"):
        relays(line - 1, 0, chain)
    with sc("own"):
        for part in range(chain):
            columns = pl.ds(part * chain_width, chain_width)

            @pl.when(z > 0)
            def _():
                chain_copy(0, z, part, z).wait_recv()
                cbuf[z, :, columns] = cbuf[z, :, columns] + pin[0, z, :, columns].astype(f32)

            @pl.when(z < line - 1)
            def _():
                chain_copy(1, z, part, z).wait_recv()
                cbuf[z, :, columns] = cbuf[z, :, columns] + pin[1, z, :, columns].astype(f32)

    out_ref[...] = cbuf[z].astype(bf16)

    for i in range(1, line):
        meta_copy(i).wait_send()

        @pl.when(z + i < line)
        def _():
            line_state_copy(i).wait_send()
            line_total_copy(i).wait_send()

    for i in range(1, plane):
        state_copy(i).wait_send()
        total_copy(i).wait_send()
        start_copy(i).wait_send()
    for h in range(2):
        away_copy(h).wait_send()
    for part in range(parts):
        for block in range(line):

            @pl.when((z >= block) & (z + 1 < line))
            def _():
                row_copy(0, block, part, z).wait_send()

            @pl.when((z <= block) & (z > 0))
            def _():
                row_copy(1, block, part, z).wait_send()

    for part in range(chain):
        for block in range(line):

            @pl.when(z != block)
            def _():
                chain_copy(0, block, part, z).wait_send()

    for j in range(line):
        for i in range(1, plane):
            select_copy(j, i).wait_send()
        partner_copy(j).wait_send()
        for h in range(halves):
            partial_copy(j, h).wait_send()
            for i in range(1, plane):
                return_copy(j, i, h).wait_send()


def run_layer(inputs, small, weights, cap):
    queries, keys, values, gates, project, residual = inputs
    decay, gain, norm, route, cos, sin = small
    count = lax.axis_size("sp")
    line = line_length(count)
    plane = count // line
    length, channels = queries.shape
    tokens, width = residual.shape
    heads, lanes = decay.shape[1], cos.shape[1]
    size = channels // heads
    groups = channels // lanes
    slice_rows = groups * size // plane
    inner = weights[0].shape[2]
    slots = plane * cap
    parts, halves, chain = 2, 2, 4
    bf16, f32 = jnp.bfloat16, jnp.float32
    dma = pltpu.SemaphoreType.DMA
    vmem = pl.BlockSpec(memory_space=pltpu.VMEM)
    hbm = pl.BlockSpec(memory_space=pl.ANY)
    return pl.pallas_call(
        functools.partial(layer_kernel, line, plane, cap, parts, halves, chain),
        out_shape=jax.ShapeDtypeStruct((tokens, width), bf16),
        in_specs=[hbm] * 4 + [vmem] * 2 + [hbm] * 2 + [vmem] * 4 + [hbm] * 3,
        out_specs=vmem,
        scratch_shapes=[
            pltpu.VMEM((length, channels), bf16),
            pltpu.VMEM((length, channels), bf16),
            pltpu.VMEM((length, channels), bf16),
            pltpu.VMEM((length, channels), bf16),
            pltpu.VMEM((channels, width), bf16),
            pltpu.VMEM((tokens, width), bf16),
            pltpu.VMEM((length, channels), f32),
            pltpu.VMEM((heads, length), f32),
            pltpu.VMEM((length, channels), bf16),
            pltpu.VMEM((length, channels), bf16),
            pltpu.VMEM((length, channels), bf16),
            pltpu.VMEM((length, channels), f32),
            pltpu.VMEM((length, channels), bf16),
            pltpu.VMEM((tokens, width), bf16),
            pltpu.VMEM((tokens, width), bf16),
            pltpu.VMEM((tokens, width), bf16),
            pltpu.VMEM(route.shape, f32),
            pltpu.VMEM((plane, slice_rows, lanes), bf16),
            pltpu.VMEM((plane, slice_rows, lanes), bf16),
            pltpu.VMEM((plane, groups, 8, lanes), f32),
            pltpu.VMEM((plane, slice_rows, lanes), f32),
            pltpu.VMEM((slice_rows, lanes), bf16),
            pltpu.VMEM((8, lanes), f32),
            pltpu.VMEM((line, slice_rows, lanes), bf16),
            pltpu.VMEM((line, 8, lanes), f32),
            pltpu.VMEM((slice_rows, lanes), f32),
            pltpu.VMEM((plane, slice_rows, lanes), bf16),
            pltpu.VMEM((plane, slice_rows, lanes), bf16),
            dma((6,)),
            dma((plane,)),
            dma((plane,)),
            dma((plane,)),
            dma((plane,)),
            dma((line, 2)),
            dma((line, 2)),
            dma((plane,)),
            dma((plane,)),
            dma((2,)),
            dma((2,)),
            pltpu.VMEM((width, inner), bf16),
            pltpu.VMEM((width, inner), bf16),
            pltpu.VMEM((inner, width), bf16),
            pltpu.VMEM((line, tokens, width), bf16),
            pltpu.VMEM((line,) + route.shape, f32),
            pltpu.VMEM((line, plane, cap, width), bf16),
            pltpu.VMEM((line, 2, plane, cap, width), bf16),
            pltpu.VMEM((2 * slots, inner), bf16),
            pltpu.VMEM((line, 2, plane, cap, width), bf16),
            pltpu.VMEM((line, plane, cap, width), bf16),
            pltpu.VMEM((line, plane, cap, width), bf16),
            pltpu.VMEM((line, plane, cap, width), bf16),
            pltpu.VMEM((line, tokens, width), f32),
            pltpu.VMEM((line, tokens, width), bf16),
            pltpu.VMEM((2, line, tokens, width), bf16),
            dma((3, 4)),
            dma((2, line, parts)),
            dma((line, parts)),
            dma((line,)),
            dma((line,)),
            dma((line, plane)),
            dma((line, plane)),
            dma((line,)),
            dma((line,)),
            dma((line, halves)),
            dma((line, halves)),
            dma((line, plane, halves)),
            dma((line, plane, halves)),
            dma((line, chain)),
            dma((2, line, chain)),
        ],
        compiler_params=pltpu.CompilerParams(
            collective_id=1, has_side_effects=True, vmem_limit_bytes=67043328
        ),
        name="layer",
    )(
        queries,
        keys,
        values,
        gates,
        decay,
        gain,
        project,
        residual,
        norm,
        route,
        cos,
        sin,
        *weights,
    )


def shards(
    queries,
    key_vectors,
    value_vectors,
    gate_inputs,
    log_decay,
    head_gain,
    out_weight,
    residual,
    norm_gain,
    expert_ids,
    expert_weights,
    gate_experts,
    up_experts,
    down_experts,
):
    tok_dev, channels = queries.shape
    head_size = channels // log_decay.shape[1]
    lanes = 128
    places = lax.axis_index("sp") * tok_dev + jnp.arange(tok_dev, dtype=jnp.int32)
    half_size = head_size // 2
    frequency = 10000.0 ** (-jnp.arange(half_size, dtype=jnp.float32) / half_size)
    angles = places.astype(jnp.float32)[:, None] * jnp.tile(frequency, lanes // half_size)
    sign = jnp.where(jnp.arange(lanes) % head_size < half_size, -1.0, 1.0)
    top_count = expert_ids.shape[1]
    route = jnp.concatenate(
        [
            expert_ids.T.astype(jnp.float32),
            expert_weights.T,
            jnp.zeros((8 - 2 * top_count, expert_ids.shape[0]), jnp.float32),
        ],
        axis=0,
    )
    return run_layer(
        (queries, key_vectors, value_vectors, gate_inputs, out_weight, residual),
        (
            log_decay,
            head_gain[None, :],
            norm_gain[None, :],
            route,
            jnp.cos(angles),
            jnp.sin(angles) * sign,
        ),
        (gate_experts, up_experts, down_experts),
        2 * tok_dev // lax.axis_size("sp"),
    )


def solution(mesh):
    return jax.shard_map(
        shards,
        mesh=mesh,
        in_specs=(
            P("sp", "tp"),
            P("sp", "tp"),
            P("sp", "tp"),
            P("sp", "tp"),
            P("sp", "tp"),
            P("tp"),
            P("tp", None),
            P(("sp", "tp"), None),
            P(),
            P(("sp", "tp"), None),
            P(("sp", "tp"), None),
            P("sp", None, "tp"),
            P("sp", None, "tp"),
            P("sp", "tp", None),
        ),
        out_specs=P(("sp", "tp"), None),
        check_vma=False,
    )
```

time: 175 us -> 123 us (0.70)
  starting transfers between devices: 20.7 us -> 0 us
  Pallas kernels: 130 us -> 115 us
  waiting for transfers between devices: 5.81 us -> 0 us
  matrix products: 5.25 us -> 0 us
  local copies, waits for them, and re-layouts: 6.4 us -> 3.53 us
  other arithmetic: 5.98 us -> 3.28 us
    ppermute x5 -> x0, starting transfers between devices: 20.7 us -> none  [the longest x4 20.7 us: shift(): lax.ppermute(packed, 'sp', [(i, i + distance) for i in range(count - dist...]
    pallas_call x1, Pallas kernels: 130 us -> 115 us  [run_layer(): pl.pallas_call(functools.partial(layer_kernel, line, plane, cap, parts, h...]
    ppermute x5 -> x0, waiting for transfers between devices: 5.81 us -> none  [the longest x4 4.76 us: shift(): lax.ppermute(packed, 'sp', [(i, i + distance) for i in range(count - dist...]
    dot_general x6 -> x0, matrix products: 5.25 us -> none  [the longest x1 1.87 us: shards(): here = jnp.dot(normed_here, out_weight, preferred_element_type=jnp.float32)]
    another operation x5 -> x0, other arithmetic: 2 us -> none
    unnamed x19 -> x2, local copies, waits for them, and re-layouts: 4.34 us -> 3.37 us
  transfers between devices with their start and end apart: 5 -> 0, of which waited for: 4 -> 0; matrix products, arithmetic and copies ran while one was open for 3% -> 0% of each run, Pallas kernels for 0% -> 0%
where the time goes in v2:
time: 123 us; the launch traced here: 122 us
  Pallas kernels  115 us (93%)
  local copies, waits for them, and re-layouts  3.53 us (3%)
  other arithmetic  3.28 us (3%)
    pallas_call x1, Pallas kernels, run_layer(): pl.pallas_call(functools.partial(layer_kernel, line, plane, cap, parts, h...  115 us
    unnamed x2, local copies, waits for them, and re-layouts  3.37 us

profile of v2, /device:TPU:0, one launch (start us, length us, event | category | flops | bytes accessed | tf_op | source)
XLA Modules:
  0.0 122.3 jit_solution(1594895151416373323)
XLA Ops:
  0.0 0.1 pad.2.clone
  0.1 0.7 convert_bitcast_fusion
  0.8 0.1 mul.28
  0.9 1.3 %maximum_maximum_fusion.route_ref = f32[8,128]{1,0:T(8,128)} fusion(f32[2,128]{1,0:T(2,128)} %bitcast.7, f32[2,128]{1,0:T(2,128)S(1)} %convert_bitcast_fusion, f32[8]{0:T(128)S(1)} %pad.2.clone), kind=kLoop, calls=%fused_computation.3 | loop fusion | flops 2048 | bytes 6176 | tf_op jit(solution)/shard_map/concatenate | solution.py:926
  2.2 1.5 %copy.15.decay_ref = f32[256,8]{1,0:T(8,128)} copy(f32[256,8]{0,1:T(8,128)} %param.18) | data formatting | bytes 16384 | tf_op args[4]
  3.7 1.2 %fusion = (f32[256,128]{1,0:T(8,128)}, f32[256,128]{1,0:T(8,128)}) fusion(f32[128]{0:T(128)S(1)} %compare_select_fusion, f32[128]{0:T(128)S(1)} %mul.28, f32[256]{0:T(256)S(1)} %add_convert_fusion), kind=kLoop, calls=%fused_computation.2 | loop fusion | flops 65536 | bytes 264192 | tf_op jit(solution)/shard_map/mul | solution.py:942
  4.9 115.4 %layer.1 = bf16[128,2048]{1,0:T(8,128)(2,1)} custom-call(bf16[256,512]{1,0:T(8,128)(2,1)} %query_hbm.1, bf16[256,512]{1,0:T(8,128)(2,1)} %key_hbm.1, bf16[256,512]{1,0:T(8,128)(2,1)} %value_hbm.1, bf16[256,512]{1,0:T(8,128)(2,1)} %gates_hbm.1, f32[256,8]{1,0:T(8,128)} %copy.15.decay_ref, f32[1,512]{1,0:T(1,128)} %bitcast.6, bf16[512,2048]{1,0:T(8,128)(2,1)} %project_hbm.1, ...), custom_call_target="tpu_custom_call" | custom-call | tf_op jit(solution)/shard_map/layer/pallas_call | solution.py:804
  120.4 1.9 %copy.17 = bf16[128,2048]{1,0:T(8,128)(2,1)} copy(bf16[128,2048]{1,0:T(8,128)(2,1)} %layer.1) | data formatting | bytes 1048576
  (5 shorter events, 0.0 us)

commit v3 on v2

--- a/solution.py
+++ b/solution.py
@@ -33,9 +33,8 @@
     project_hbm,
     residual_hbm,
     norm_ref,
-    route_ref,
-    cos_ref,
-    sin_ref,
+    ids_ref,
+    shares_ref,
     gate_hbm,
     up_hbm,
     down_hbm,
@@ -46,6 +45,8 @@
     gates_ref,
     project_ref,
     residual_ref,
+    cos_ref,
+    sin_ref,
     running_ref,
     by_head_ref,
     turned_query,
@@ -115,7 +116,7 @@
     length, channels = query_ref.shape
     tokens, width = residual_ref.shape
     lanes = cos_ref.shape[1]
-    heads = decay_ref.shape[1]
+    heads = decay_ref.shape[0]
     size = channels // heads
     pack = lanes // size
     groups = channels // lanes
@@ -189,81 +190,111 @@
         return value
 
     count = line * plane
-    expert = lax.broadcasted_iota(jnp.int32, (count, tokens), 0).astype(f32)
-    first_hot = jnp.where(expert == route_ref[0:1, :], 1.0, 0.0)
-    second_hot = jnp.where(expert == route_ref[1:2, :], 1.0, 0.0)
-    earlier = lax.broadcasted_iota(jnp.int32, (tokens, tokens), 0) < (
-        lax.broadcasted_iota(jnp.int32, (tokens, tokens), 1)
-    )
-    taken = jnp.dot(
-        (first_hot + second_hot).astype(bf16),
-        jnp.where(earlier, 1.0, 0.0).astype(bf16),
-        preferred_element_type=f32,
-    )
-    first_rank = jnp.sum(first_hot * taken, axis=0, keepdims=True)
-    second_rank = jnp.sum(second_hot * taken, axis=0, keepdims=True)
-    meta_ref[...] = route_ref[...]
-    meta_ref[0:1, :] = route_ref[0:1, :] * cap + first_rank
-    meta_ref[1:2, :] = route_ref[1:2, :] * cap + second_rank
-
-    rows_of = lax.broadcasted_iota(jnp.int32, (length, length), 0)
-    columns_of = lax.broadcasted_iota(jnp.int32, (length, length), 1)
-    causal = rows_of >= columns_of
-    lower = jnp.where(causal, 1.0, 0.0).astype(bf16)
-    upper = jnp.where(rows_of <= columns_of, 1.0, 0.0).astype(bf16)
-    spread = lax.broadcasted_iota(jnp.int32, (heads, channels), 1) // size == (
-        lax.broadcasted_iota(jnp.int32, (heads, channels), 0)
-    )
-    spread = jnp.where(spread, 1.0, 0.0).astype(bf16)
-    rest = decay_ref[...]
-    running, by_head = 0.0, 0.0
-    for _ in range(3):
-        piece = rest.astype(bf16)
-        rest = rest - piece.astype(f32)
-        wide_piece = jnp.dot(piece, spread, preferred_element_type=f32).astype(bf16)
-        running = running + jnp.dot(lower, wide_piece, preferred_element_type=f32)
-        by_head = by_head + lax.dot_general(piece, upper, upright, preferred_element_type=f32)
-    running_ref[...] = running
-    by_head_ref[...] = by_head
+    with jax.named_scope("slots"):
+        expert = lax.broadcasted_iota(jnp.int32, (count, tokens), 0).astype(f32)
+        first, second = ids_ref[0:1, :].astype(f32), ids_ref[1:2, :].astype(f32)
+        first_hot = jnp.where(expert == first, 1.0, 0.0)
+        second_hot = jnp.where(expert == second, 1.0, 0.0)
+        earlier = lax.broadcasted_iota(jnp.int32, (tokens, tokens), 0) < (
+            lax.broadcasted_iota(jnp.int32, (tokens, tokens), 1)
+        )
+        taken = jnp.dot(
+            (first_hot + second_hot).astype(bf16),
+            jnp.where(earlier, 1.0, 0.0).astype(bf16),
+            preferred_element_type=f32,
+        )
+        first_rank = jnp.sum(first_hot * taken, axis=0, keepdims=True)
+        second_rank = jnp.sum(second_hot * taken, axis=0, keepdims=True)
+        meta_ref[...] = jnp.zeros_like(meta_ref)
+        meta_ref[0:1, :] = first * cap + first_rank
+        meta_ref[1:2, :] = second * cap + second_rank
+        meta_ref[2:4, :] = shares_ref[...]
+
+    with jax.named_scope("running"):
+        rows_of = lax.broadcasted_iota(jnp.int32, (length, length), 0)
+        columns_of = lax.broadcasted_iota(jnp.int32, (length, length), 1)
+        causal = rows_of >= columns_of
+        lower = jnp.where(causal, 1.0, 0.0).astype(bf16)
+        upper = jnp.where(rows_of <= columns_of, 1.0, 0.0).astype(bf16)
+        spread = lax.broadcasted_iota(jnp.int32, (heads, channels), 1) // size == (
+            lax.broadcasted_iota(jnp.int32, (heads, channels), 0)
+        )
+        spread = jnp.where(spread, 1.0, 0.0).astype(bf16)
+        rest = decay_ref[...]
+        running, by_head = 0.0, 0.0
+        for _ in range(3):
+            piece = rest.astype(bf16)
+            rest = rest - piece.astype(f32)
+            wide_piece = lax.dot_general(piece, spread, upright, preferred_element_type=f32)
+            wide_piece = wide_piece.astype(bf16)
+            running = running + jnp.dot(lower, wide_piece, preferred_element_type=f32)
+            by_head = by_head + jnp.dot(piece, upper, preferred_element_type=f32)
+        running_ref[...] = running
+        by_head_ref[...] = by_head
 
     swapped = lax.broadcasted_iota(jnp.int32, (lanes, lanes), 0) == (
         lax.broadcasted_iota(jnp.int32, (lanes, lanes), 1) ^ (size // 2)
     )
     swapped = jnp.where(swapped, 1.0, 0.0).astype(bf16)
-    for copy in loads[:3]:
-        copy.wait()
+    with jax.named_scope("table"):
+        half_size = size // 2
+        step_of = lane % half_size
+        frequency = jnp.zeros((1, lanes), f32)
+        for number in range(half_size):
+            constant = float(10000.0 ** (-number / half_size))
+            frequency = jnp.where(step_of == number, constant, frequency)
+        fine = 16
+        row = lax.broadcasted_iota(jnp.int32, (fine, lanes), 0)
+        near_angle = row.astype(f32) * frequency
+        near_cos, near_sin = jnp.cos(near_angle), jnp.sin(near_angle)
+        rounds = length // fine
+        row = lax.broadcasted_iota(jnp.int32, (rounds, lanes), 0)
+        far_angle = (sp * length + row * fine).astype(f32) * frequency
+        far_cos, far_sin = jnp.cos(far_angle), jnp.sin(far_angle)
+        sign = jnp.where(lane % size < half_size, -1.0, 1.0)
+        for number in range(rounds):
+            some = pl.ds(number * fine, fine)
+            a, b = far_cos[number : number + 1, :], far_sin[number : number + 1, :]
+            cos_ref[some, :] = a * near_cos - b * near_sin
+            sin_ref[some, :] = (b * near_cos + a * near_sin) * sign
+
+    with jax.named_scope("loadw"):
+        for copy in loads[:3]:
+            copy.wait()
 
     def turn(block):
         other = jnp.dot(block, swapped, preferred_element_type=f32)
         return block.astype(f32) * cos_ref[...] + other * sin_ref[...]
 
-    for group in range(groups):
-        where = pl.ds(group * lanes, lanes)
-        run = running_ref[:, where]
-        query = turn(query_ref[:, where])
-        key = turn(key_ref[:, where]) * size ** (-0.5)
-        turned_query[:, where] = query.astype(bf16)
-        turned_key[:, where] = key.astype(bf16)
-        start_query[:, where] = (query * jnp.exp(run)).astype(bf16)
-        end = run[length - 1 : length, :]
-        final = lax.dot_general(
-            (key * jnp.exp(end - run)).astype(bf16),
-            value_ref[:, where],
-            upright,
-            preferred_element_type=f32,
-        )
-        state = by_lane([final[n * size : (n + 1) * size, :] for n in range(pack)])
-        totals[p, group] = jnp.broadcast_to(end, totals.shape[2:])
-        per = size // slice_rows if slice_rows < size else 1
-        deep = min(slice_rows, size)
-        for part in range(per):
-            row = group * size + part * deep
-            state_out[row // slice_rows, pl.ds(row % slice_rows, deep), :] = state[
-                part * deep : (part + 1) * deep, :
-            ].astype(bf16)
-    state_in[p] = state_out[p]
-
-    pl.semaphore_wait(barrier, len(peers))
+    with jax.named_scope("turn"):
+        for group in range(groups):
+            where = pl.ds(group * lanes, lanes)
+            run = running_ref[:, where]
+            query = turn(query_ref[:, where])
+            key = turn(key_ref[:, where]) * size ** (-0.5)
+            turned_query[:, where] = query.astype(bf16)
+            turned_key[:, where] = key.astype(bf16)
+            start_query[:, where] = (query * jnp.exp(run)).astype(bf16)
+            end = run[length - 1 : length, :]
+            final = lax.dot_general(
+                (key * jnp.exp(end - run)).astype(bf16),
+                value_ref[:, where],
+                upright,
+                preferred_element_type=f32,
+            )
+            state = by_lane([final[n * size : (n + 1) * size, :] for n in range(pack)])
+            totals[p, group] = jnp.broadcast_to(end, totals.shape[2:])
+            per = size // slice_rows if slice_rows < size else 1
+            deep = min(slice_rows, size)
+            for part in range(per):
+                row = group * size + part * deep
+                state_out[row // slice_rows, pl.ds(row % slice_rows, deep), :] = state[
+                    part * deep : (part + 1) * deep, :
+                ].astype(bf16)
+        state_in[p] = state_out[p]
+
+    with jax.named_scope("barrier"):
+        pl.semaphore_wait(barrier, len(peers))
 
     def state_copy(i):
         q = lax.rem(p + i, plane)
@@ -310,12 +341,15 @@
                 )
             within_ref[:, where] = by_lane(total)
 
-    attend(0, groups // 2)
+    with jax.named_scope("attendA"):
+        attend(0, groups // 2)
 
     mine = p * slice_rows // size
-    for i in range(1, plane):
-        state_copy(i).wait_recv()
-        total_copy(i).wait_recv()
+    with jax.named_scope("wait1"):
+        for i in range(1, plane):
+            state_copy(i).wait_recv()
+            total_copy(i).wait_recv()
+
     held = jnp.zeros((slice_rows, lanes), f32)
     elapsed = jnp.zeros((1, lanes), f32)
     for q in range(plane):
@@ -343,17 +377,19 @@
             line_state_copy(i).start()
             line_total_copy(i).start()
 
-    attend(groups // 2, groups)
-
-    carry_ref[...] = jnp.zeros_like(carry_ref)
-    for i in range(line - 1, 0, -1):
-
-        @pl.when(z >= i)
-        def _():
-            line_state_copy(i).wait_recv()
-            line_total_copy(i).wait_recv()
-            step = line_total[z - i][0:1, :]
-            carry_ref[...] = jnp.exp(step) * carry_ref[...] + line_state[z - i].astype(f32)
+    with jax.named_scope("attendB"):
+        attend(groups // 2, groups)
+
+    with jax.named_scope("wait2"):
+        carry_ref[...] = jnp.zeros_like(carry_ref)
+        for i in range(line - 1, 0, -1):
+
+            @pl.when(z >= i)
+            def _():
+                line_state_copy(i).wait_recv()
+                line_total_copy(i).wait_recv()
+                step = line_total[z - i][0:1, :]
+                carry_ref[...] = jnp.exp(step) * carry_ref[...] + line_state[z - i].astype(f32)
 
     elapsed = jnp.zeros((1, lanes), f32)
     for q in range(plane):
@@ -370,45 +406,47 @@
     for i in range(1, plane):
         start_copy(i).start()
     start_state[p] = back_state[p]
-    for copy in loads[3:]:
-        copy.wait()
-    for i in range(1, plane):
-        start_copy(i).wait_recv()
-
-    for group in range(groups):
-        where = pl.ds(group * lanes, lanes)
-        pieces = []
-        for part in range(max(1, size // slice_rows)):
-            row = group * size + part * slice_rows
-            deep = min(slice_rows, size)
-            pieces.append(start_state[row // slice_rows, pl.ds(row % slice_rows, deep), :])
-        state = pieces[0] if len(pieces) == 1 else jnp.concatenate(pieces, axis=0)
-        diagonal = jnp.concatenate(
-            [
-                jnp.where(
-                    (lane >= n * size) & (lane < (n + 1) * size), state, jnp.zeros_like(state)
+    with jax.named_scope("wait3"):
+        for copy in loads[3:]:
+            copy.wait()
+        for i in range(1, plane):
+            start_copy(i).wait_recv()
+
+    with jax.named_scope("epilogue"):
+        for group in range(groups):
+            where = pl.ds(group * lanes, lanes)
+            pieces = []
+            for part in range(max(1, size // slice_rows)):
+                row = group * size + part * slice_rows
+                deep = min(slice_rows, size)
+                pieces.append(start_state[row // slice_rows, pl.ds(row % slice_rows, deep), :])
+            state = pieces[0] if len(pieces) == 1 else jnp.concatenate(pieces, axis=0)
+            diagonal = jnp.concatenate(
+                [
+                    jnp.where(
+                        (lane >= n * size) & (lane < (n + 1) * size), state, jnp.zeros_like(state)
+                    )
+                    for n in range(pack)
+                ],
+                axis=0,
+            )
+            retained = within_ref[:, where] + jnp.dot(
+                start_query[:, where], diagonal, preferred_element_type=f32
+            )
+            square = retained * retained
+            sums = [
+                jnp.sum(
+                    jnp.where((lane >= n * size) & (lane < (n + 1) * size), square, 0.0),
+                    axis=1,
+                    keepdims=True,
                 )
                 for n in range(pack)
-            ],
-            axis=0,
-        )
-        retained = within_ref[:, where] + jnp.dot(
-            start_query[:, where], diagonal, preferred_element_type=f32
-        )
-        square = retained * retained
-        sums = [
-            jnp.sum(
-                jnp.where((lane >= n * size) & (lane < (n + 1) * size), square, 0.0),
-                axis=1,
-                keepdims=True,
-            )
-            for n in range(pack)
-        ]
-        mean = by_lane(sums) * (1.0 / size)
-        gates = gates_ref[:, where].astype(f32)
-        normed = retained * lax.rsqrt(mean + 1e-06) * gain_ref[:, where]
-        normed = normed * (gates / (1.0 + jnp.exp(-gates)))
-        normed_ref[:, where] = normed.astype(bf16)
+            ]
+            mean = by_lane(sums) * (1.0 / size)
+            gates = gates_ref[:, where].astype(f32)
+            normed = retained * lax.rsqrt(mean + 1e-06) * gain_ref[:, where]
+            normed = normed * (gates / (1.0 + jnp.exp(-gates)))
+            normed_ref[:, where] = normed.astype(bf16)
 
     def away_copy(h):
         columns = pl.ds(h * (width // 2), width // 2)
@@ -418,29 +456,30 @@
 
     away_rows = pl.ds(pl.multiple_of((1 - core) * tokens, tokens), tokens)
     here_rows = pl.ds(pl.multiple_of(core * tokens, tokens), tokens)
-    for h in range(2):
-        columns = pl.ds(h * (width // 2), width // 2)
-        away_ref[:, columns] = jnp.dot(
-            normed_ref[away_rows, :], project_ref[:, columns], preferred_element_type=f32
-        ).astype(bf16)
-        away_copy(h).start()
-    squares = jnp.zeros((tokens, 1), f32)
-    for h in range(2):
-        columns = pl.ds(h * (width // 2), width // 2)
-        here = jnp.dot(
-            normed_ref[here_rows, :], project_ref[:, columns], preferred_element_type=f32
-        ).astype(bf16)
-        away_copy(h).wait_recv()
-        projected = here.astype(f32) + got_ref[:, columns].astype(f32)
-        mixed = (residual_ref[:, columns].astype(f32) + projected).astype(bf16)
-        mixed_ref[:, columns] = mixed
-        mixed = mixed.astype(f32)
-        squares = squares + jnp.sum(mixed * mixed, axis=1, keepdims=True)
-    scale = lax.rsqrt(squares * (1.0 / width) + 1e-06)
-    for h in range(2):
-        columns = pl.ds(h * (width // 2), width // 2)
-        normed = mixed_ref[:, columns].astype(f32) * scale * norm_ref[:, columns]
-        zbuf[z, :, columns] = normed.astype(bf16)
+    with jax.named_scope("proj"):
+        for h in range(2):
+            columns = pl.ds(h * (width // 2), width // 2)
+            away_ref[:, columns] = jnp.dot(
+                normed_ref[away_rows, :], project_ref[:, columns], preferred_element_type=f32
+            ).astype(bf16)
+            away_copy(h).start()
+        squares = jnp.zeros((tokens, 1), f32)
+        for h in range(2):
+            columns = pl.ds(h * (width // 2), width // 2)
+            here = jnp.dot(
+                normed_ref[here_rows, :], project_ref[:, columns], preferred_element_type=f32
+            ).astype(bf16)
+            away_copy(h).wait_recv()
+            projected = here.astype(f32) + got_ref[:, columns].astype(f32)
+            mixed = (residual_ref[:, columns].astype(f32) + projected).astype(bf16)
+            mixed_ref[:, columns] = mixed
+            mixed = mixed.astype(f32)
+            squares = squares + jnp.sum(mixed * mixed, axis=1, keepdims=True)
+        scale = lax.rsqrt(squares * (1.0 / width) + 1e-06)
+        for h in range(2):
+            columns = pl.ds(h * (width // 2), width // 2)
+            normed = mixed_ref[:, columns].astype(f32) * scale * norm_ref[:, columns]
+            zbuf[z, :, columns] = normed.astype(bf16)
 
     piece_rows = tokens // parts
     chain_width = width // chain
@@ -504,6 +543,12 @@
         q = lax.rem(p + i, plane)
         return remote(
             sel.at[j, q], xbuf.at[j, core, p], psend.at[j, i], precv.at[j, i], at(z, q)
+        )
+
+    def partner_copy(j, i):
+        q = lax.rem(p + plane - i, plane)
+        return remote(
+            xbuf.at[j, core, q], xbuf.at[j, core, q], tsend.at[j, i], trecv.at[j, i], partner
         )
 
     def select(j):
@@ -516,16 +561,12 @@
         for i in range(1, plane):
             select_copy(j, i).start()
         xbuf[j, core, p] = sel[j, p]
-
-    def partner_copy(j):
-        return remote(
-            xbuf.at[j, core], xbuf.at[j, core], tsend.at[j], trecv.at[j], partner
-        )
+        partner_copy(j, 0).start()
 
     def collect(j):
         for i in range(1, plane):
             select_copy(j, i).wait_recv()
-        partner_copy(j).start()
+            partner_copy(j, i).start()
 
     half = width // halves
 
@@ -550,17 +591,15 @@
         else:
             batch = xbuf[j].astype(f32).reshape(tall, width).astype(bf16)
 
-        @pl.loop(lo, hi)
-        def _(tile):
-            columns = pl.ds(pl.multiple_of(tile * wide, wide), wide)
+        for tile in range(lo, hi):
+            columns = pl.ds(tile * wide, wide)
             gate = jnp.dot(batch, gate_ref[:, columns], preferred_element_type=f32)
             up = jnp.dot(batch, up_ref[:, columns], preferred_element_type=f32)
             hidden[:, columns] = (gate * up / (1.0 + jnp.exp(-gate))).astype(bf16)
 
     def narrow(j, h):
-        @pl.loop(h * (half // wide), (h + 1) * (half // wide))
-        def _(tile):
-            columns = pl.ds(pl.multiple_of(tile * wide, wide), wide)
+        for tile in range(h * (half // wide), (h + 1) * (half // wide)):
+            columns = pl.ds(tile * wide, wide)
             value = jnp.dot(hidden[...], down_ref[:, columns], preferred_element_type=f32)
             ybuf[j, :, :, :, columns] = value.reshape(2, plane, cap, wide).astype(bf16)
 
@@ -675,9 +714,10 @@
         collect(0)
     for j in range(line):
         last = j + 1 == line
-        cut = max(0, tiles - j * tiles // 2)
+        cut = tiles if last else (tiles + j) // 2
         with sc(f"xwait#{j}"):
-            partner_copy(j).wait_recv()
+            for i in range(plane):
+                partner_copy(j, i).wait_recv()
             if j == 0:
                 for copy in weights:
                     copy.wait()
@@ -690,25 +730,35 @@
                 select(j + 1)
         with sc(f"widen#{j}b"):
             widen(j, cut, tiles)
-        if j >= 1:
+        if j >= 2 and last:
             with sc(f"combine#{j - 1}"):
                 weigh = weigh_of(j - 1)
                 for h in range(halves):
                     combine(j - 1, h, weigh)
         with sc(f"narrow#{j}a"):
             narrow(j, 0)
+        if j >= 2 and not last:
+            with sc(f"combine#{j - 1}"):
+                weigh = weigh_of(j - 1)
+                for h in range(halves):
+                    combine(j - 1, h, weigh)
         with sc(f"narrow#{j}b"):
             for h in range(1, halves):
                 narrow(j, h)
         if j + 2 < line:
             with sc(f"pass#{j + 2}a"):
                 pass_on(j + 2, 0, parts // 2)
+        if j >= 1:
+            with sc(f"give#{j}"):
+                for h in range(halves):
+                    give_back(j, h)
+        if j == max(0, line - 2):
+            with sc("give#0"):
+                for h in range(halves):
+                    give_back(0, h)
         if not last:
             with sc(f"collect#{j + 1}"):
                 collect(j + 1)
-        with sc(f"give#{j}"):
-            for h in range(halves):
-                give_back(j, h)
         if 2 <= j < line - 2:
             relays(j, 0, chain)
     weigh = weigh_of(line - 1)
@@ -724,6 +774,10 @@
                 relays(line - 2, h * share + share // 2, (h + 1) * share)
     with sc("relays#c"):
         relays(line - 1, 0, chain)
+    with sc("combine#own"):
+        weigh = weigh_of(0)
+        for h in range(halves):
+            combine(0, h, weigh)
     with sc("own"):
         for part in range(chain):
             columns = pl.ds(part * chain_width, chain_width)
@@ -775,7 +829,8 @@
     for j in range(line):
         for i in range(1, plane):
             select_copy(j, i).wait_send()
-        partner_copy(j).wait_send()
+        for i in range(plane):
+            partner_copy(j, i).wait_send()
         for h in range(halves):
             partial_copy(j, h).wait_send()
             for i in range(1, plane):
@@ -784,13 +839,14 @@
 
 def run_layer(inputs, small, weights, cap):
     queries, keys, values, gates, project, residual = inputs
-    decay, gain, norm, route, cos, sin = small
+    decay, gain, norm, ids, shares = small
+    lanes = 128
     count = lax.axis_size("sp")
     line = line_length(count)
     plane = count // line
     length, channels = queries.shape
     tokens, width = residual.shape
-    heads, lanes = decay.shape[1], cos.shape[1]
+    heads = decay.shape[0]
     size = channels // heads
     groups = channels // lanes
     slice_rows = groups * size // plane
@@ -804,7 +860,7 @@
     return pl.pallas_call(
         functools.partial(layer_kernel, line, plane, cap, parts, halves, chain),
         out_shape=jax.ShapeDtypeStruct((tokens, width), bf16),
-        in_specs=[hbm] * 4 + [vmem] * 2 + [hbm] * 2 + [vmem] * 4 + [hbm] * 3,
+        in_specs=[hbm] * 4 + [vmem] * 2 + [hbm] * 2 + [vmem] * 3 + [hbm] * 3,
         out_specs=vmem,
         scratch_shapes=[
             pltpu.VMEM((length, channels), bf16),
@@ -813,6 +869,8 @@
             pltpu.VMEM((length, channels), bf16),
             pltpu.VMEM((channels, width), bf16),
             pltpu.VMEM((tokens, width), bf16),
+            pltpu.VMEM((length, lanes), f32),
+            pltpu.VMEM((length, lanes), f32),
             pltpu.VMEM((length, channels), f32),
             pltpu.VMEM((heads, length), f32),
             pltpu.VMEM((length, channels), bf16),
@@ -823,7 +881,7 @@
             pltpu.VMEM((tokens, width), bf16),
             pltpu.VMEM((tokens, width), bf16),
             pltpu.VMEM((tokens, width), bf16),
-            pltpu.VMEM(route.shape, f32),
+            pltpu.VMEM((8, tokens), f32),
             pltpu.VMEM((plane, slice_rows, lanes), bf16),
             pltpu.VMEM((plane, slice_rows, lanes), bf16),
             pltpu.VMEM((plane, groups, 8, lanes), f32),
@@ -850,7 +908,7 @@
             pltpu.VMEM((width, inner), bf16),
             pltpu.VMEM((inner, width), bf16),
             pltpu.VMEM((line, tokens, width), bf16),
-            pltpu.VMEM((line,) + route.shape, f32),
+            pltpu.VMEM((line, 8, tokens), f32),
             pltpu.VMEM((line, plane, cap, width), bf16),
             pltpu.VMEM((line, 2, plane, cap, width), bf16),
             pltpu.VMEM((2 * slots, inner), bf16),
@@ -868,8 +926,8 @@
             dma((line,)),
             dma((line, plane)),
             dma((line, plane)),
-            dma((line,)),
-            dma((line,)),
+            dma((line, plane)),
+            dma((line, plane)),
             dma((line, halves)),
             dma((line, halves)),
             dma((line, plane, halves)),
@@ -891,9 +949,8 @@
         project,
         residual,
         norm,
-        route,
-        cos,
-        sin,
+        ids,
+        shares,
         *weights,
     )
 
@@ -914,35 +971,11 @@
     up_experts,
     down_experts,
 ):
-    tok_dev, channels = queries.shape
-    head_size = channels // log_decay.shape[1]
-    lanes = 128
-    places = lax.axis_index("sp") * tok_dev + jnp.arange(tok_dev, dtype=jnp.int32)
-    half_size = head_size // 2
-    frequency = 10000.0 ** (-jnp.arange(half_size, dtype=jnp.float32) / half_size)
-    angles = places.astype(jnp.float32)[:, None] * jnp.tile(frequency, lanes // half_size)
-    sign = jnp.where(jnp.arange(lanes) % head_size < half_size, -1.0, 1.0)
-    top_count = expert_ids.shape[1]
-    route = jnp.concatenate(
-        [
-            expert_ids.T.astype(jnp.float32),
-            expert_weights.T,
-            jnp.zeros((8 - 2 * top_count, expert_ids.shape[0]), jnp.float32),
-        ],
-        axis=0,
-    )
     return run_layer(
         (queries, key_vectors, value_vectors, gate_inputs, out_weight, residual),
-        (
-            log_decay,
-            head_gain[None, :],
-            norm_gain[None, :],
-            route,
-            jnp.cos(angles),
-            jnp.sin(angles) * sign,
-        ),
+        (log_decay.T, head_gain[None, :], norm_gain[None, :], expert_ids.T, expert_weights.T),
         (gate_experts, up_experts, down_experts),
-        2 * tok_dev // lax.axis_size("sp"),
+        2 * queries.shape[0] // lax.axis_size("sp"),
     )
 
 

time: 123 us -> 111 us (0.902)
  Pallas kernels: 115 us -> 109 us
  other arithmetic: 3.28 us -> 0 us
  local copies, waits for them, and re-layouts: 3.53 us -> 1.88 us
    pallas_call x1, Pallas kernels: 115 us -> 109 us  [run_layer(): pl.pallas_call(functools.partial(layer_kernel, line, plane, cap, parts, h...]
    unnamed x2 -> x1, local copies, waits for them, and re-layouts: 3.37 us -> 1.88 us
    concatenate x1 -> x0, other arithmetic: 1.34 us -> none  [shards(): jnp.concatenate([expert_ids.T.astype(jnp.float32), expert_weights.T, jnp....]
    mul x1 -> x0, other arithmetic: 1.24 us -> none  [shards(): jnp.sin(angles) * sign]
where the time goes in v3:
time: 111 us
  Pallas kernels  109 us (98%)
  local copies, waits for them, and re-layouts  1.88 us (2%)
    pallas_call x1, Pallas kernels, run_layer(): pl.pallas_call(functools.partial(layer_kernel, line, plane, cap, parts, h...  109 us

profile of v3, /device:TPU:0, one launch (start us, length us, event | category | flops | bytes accessed | tf_op | source)
XLA Modules:
  0.0 111.2 jit_solution(18367080755245843505)
XLA Ops:
  0.0 109.3 %layer.1 = bf16[128,2048]{1,0:T(8,128)(2,1)} custom-call(bf16[256,512]{1,0:T(8,128)(2,1)} %query_hbm.1, bf16[256,512]{1,0:T(8,128)(2,1)} %key_hbm.1, bf16[256,512]{1,0:T(8,128)(2,1)} %value_hbm.1, bf16[256,512]{1,0:T(8,128)(2,1)} %gates_hbm.1, f32[8,256]{1,0:T(8,128)} %bitcast.5, f32[1,512]{1,0:T(1,128)} %bitcast.7, bf16[512,2048]{1,0:T(8,128)(2,1)} %project_hbm.1, ...), custom_call_target="tpu_custom_call" | custom-call | tf_op jit(solution)/shard_map/layer/pallas_call | solution.py:860
  109.3 1.9 %copy.16 = bf16[128,2048]{1,0:T(8,128)(2,1)} copy(bf16[128,2048]{1,0:T(8,128)(2,1)} %layer.1) | data formatting | bytes 1048576

commit v4 on v3

--- a/solution.py
+++ b/solution.py
@@ -70,6 +70,7 @@
     back_state,
     start_state,
     lsem,
+    osem,
     asend,
     arecv,
     bsend,
@@ -139,6 +140,13 @@
             device_id_type=MESH,
         )
 
+    def sent(ref, semaphore):
+        remote(ref, ref, semaphore, semaphore, partner).wait_send()
+
+    def came(ref, semaphore):
+        remote(ref, ref, semaphore, semaphore, partner).wait_recv()
+
+    others = pl.ds(0, plane - 1)
     loads = [
         pltpu.make_async_copy(source, target, lsem.at[number])
         for number, (source, target) in enumerate(
@@ -155,18 +163,12 @@
     for copy in loads:
         copy.start()
 
-    weights = []
-    for number, (source, target) in enumerate(
-        ((gate_hbm, gate_ref), (up_hbm, up_ref), (down_hbm, down_ref))
-    ):
-        depth = target.shape[0] // 4
-        for piece in range(4):
-            part = pl.ds(piece * depth, depth)
-            weights.append(
-                pltpu.make_async_copy(
-                    source.at[0, part], target.at[part], wsem.at[number, piece]
-                )
-            )
+    weights = [
+        pltpu.make_async_copy(source.at[0], target, wsem.at[number])
+        for number, (source, target) in enumerate(
+            ((gate_hbm, gate_ref), (up_hbm, up_ref), (down_hbm, down_ref))
+        )
+    ]
 
     barrier = pltpu.get_barrier_semaphore()
     peers = [at(lax.rem(z + i, line), p) for i in range(1, line)]
@@ -188,27 +190,6 @@
         for number in range(pack - 2, -1, -1):
             value = jnp.where(lane < (number + 1) * size, pieces[number], value)
         return value
-
-    count = line * plane
-    with jax.named_scope("slots"):
-        expert = lax.broadcasted_iota(jnp.int32, (count, tokens), 0).astype(f32)
-        first, second = ids_ref[0:1, :].astype(f32), ids_ref[1:2, :].astype(f32)
-        first_hot = jnp.where(expert == first, 1.0, 0.0)
-        second_hot = jnp.where(expert == second, 1.0, 0.0)
-        earlier = lax.broadcasted_iota(jnp.int32, (tokens, tokens), 0) < (
-            lax.broadcasted_iota(jnp.int32, (tokens, tokens), 1)
-        )
-        taken = jnp.dot(
-            (first_hot + second_hot).astype(bf16),
-            jnp.where(earlier, 1.0, 0.0).astype(bf16),
-            preferred_element_type=f32,
-        )
-        first_rank = jnp.sum(first_hot * taken, axis=0, keepdims=True)
-        second_rank = jnp.sum(second_hot * taken, axis=0, keepdims=True)
-        meta_ref[...] = jnp.zeros_like(meta_ref)
-        meta_ref[0:1, :] = first * cap + first_rank
-        meta_ref[1:2, :] = second * cap + second_rank
-        meta_ref[2:4, :] = shares_ref[...]
 
     with jax.named_scope("running"):
         rows_of = lax.broadcasted_iota(jnp.int32, (length, length), 0)
@@ -299,12 +280,12 @@
     def state_copy(i):
         q = lax.rem(p + i, plane)
         return remote(
-            state_out.at[q], state_in.at[p], asend.at[i], arecv.at[i], at(z, q)
+            state_out.at[q], state_in.at[p], asend.at[0], arecv.at[0], at(z, q)
         )
 
     def total_copy(i):
         q = lax.rem(p + i, plane)
-        return remote(totals.at[p], totals.at[p], bsend.at[i], brecv.at[i], at(z, q))
+        return remote(totals.at[p], totals.at[p], bsend.at[0], brecv.at[0], at(z, q))
 
     for i in range(1, plane):
         state_copy(i).start()
@@ -312,8 +293,29 @@
 
     def meta_copy(i):
         return remote(
-            meta_ref, meta.at[z], msend.at[i], mrecv.at[i], at(lax.rem(z + i, line), p)
-        )
+            meta_ref, meta.at[z], msend.at[0], mrecv.at[0], at(lax.rem(z + i, line), p)
+        )
+
+    count = line * plane
+    with jax.named_scope("slots"):
+        expert = lax.broadcasted_iota(jnp.int32, (count, tokens), 0).astype(f32)
+        first, second = ids_ref[0:1, :].astype(f32), ids_ref[1:2, :].astype(f32)
+        first_hot = jnp.where(expert == first, 1.0, 0.0)
+        second_hot = jnp.where(expert == second, 1.0, 0.0)
+        earlier = lax.broadcasted_iota(jnp.int32, (tokens, tokens), 0) < (
+            lax.broadcasted_iota(jnp.int32, (tokens, tokens), 1)
+        )
+        taken = jnp.dot(
+            (first_hot + second_hot).astype(bf16),
+            jnp.where(earlier, 1.0, 0.0).astype(bf16),
+            preferred_element_type=f32,
+        )
+        first_rank = jnp.sum(first_hot * taken, axis=0, keepdims=True)
+        second_rank = jnp.sum(second_hot * taken, axis=0, keepdims=True)
+        meta_ref[...] = jnp.zeros_like(meta_ref)
+        meta_ref[0:1, :] = first * cap + first_rank
+        meta_ref[1:2, :] = second * cap + second_rank
+        meta_ref[2:4, :] = shares_ref[...]
 
     for i in range(1, line):
         meta_copy(i).start()
@@ -346,9 +348,8 @@
 
     mine = p * slice_rows // size
     with jax.named_scope("wait1"):
-        for i in range(1, plane):
-            state_copy(i).wait_recv()
-            total_copy(i).wait_recv()
+        came(state_in.at[others], arecv.at[0])
+        came(totals.at[others], brecv.at[0])
 
     held = jnp.zeros((slice_rows, lanes), f32)
     elapsed = jnp.zeros((1, lanes), f32)
@@ -362,12 +363,12 @@
 
     def line_state_copy(i):
         return remote(
-            plane_state, line_state.at[z], ctsend.at[i, 0], ctrecv.at[i, 0], at(z + i, p)
+            plane_state, line_state.at[z], ctsend.at[0], ctrecv.at[i, 0], at(z + i, p)
         )
 
     def line_total_copy(i):
         return remote(
-            plane_total, line_total.at[z], ctsend.at[i, 1], ctrecv.at[i, 1], at(z + i, p)
+            plane_total, line_total.at[z], ctsend.at[1], ctrecv.at[i, 1], at(z + i, p)
         )
 
     for i in range(1, line):
@@ -400,7 +401,7 @@
     def start_copy(i):
         q = lax.rem(p + i, plane)
         return remote(
-            back_state.at[q], start_state.at[p], dsend.at[i], drecv.at[i], at(z, q)
+            back_state.at[q], start_state.at[p], dsend.at[0], drecv.at[0], at(z, q)
         )
 
     for i in range(1, plane):
@@ -409,8 +410,7 @@
     with jax.named_scope("wait3"):
         for copy in loads[3:]:
             copy.wait()
-        for i in range(1, plane):
-            start_copy(i).wait_recv()
+        came(start_state.at[others], drecv.at[0])
 
     with jax.named_scope("epilogue"):
         for group in range(groups):
@@ -451,7 +451,7 @@
     def away_copy(h):
         columns = pl.ds(h * (width // 2), width // 2)
         return remote(
-            away_ref.at[:, columns], got_ref.at[:, columns], esend.at[h], erecv.at[h], partner
+            away_ref.at[:, columns], got_ref.at[:, columns], esend.at[0], erecv.at[h], partner
         )
 
     away_rows = pl.ds(pl.multiple_of((1 - core) * tokens, tokens), tokens)
@@ -489,7 +489,7 @@
         return remote(
             zbuf.at[block, rows],
             zbuf.at[block, rows],
-            zsend.at[way, block, part],
+            zsend.at[way],
             zrecv.at[block, part],
             at(target, p),
         )
@@ -542,13 +542,13 @@
     def select_copy(j, i):
         q = lax.rem(p + i, plane)
         return remote(
-            sel.at[j, q], xbuf.at[j, core, p], psend.at[j, i], precv.at[j, i], at(z, q)
+            sel.at[j, q], xbuf.at[j, core, p], psend.at[0], precv.at[j, i], at(z, q)
         )
 
     def partner_copy(j, i):
         q = lax.rem(p + plane - i, plane)
         return remote(
-            xbuf.at[j, core, q], xbuf.at[j, core, q], tsend.at[j, i], trecv.at[j, i], partner
+            xbuf.at[j, core, q], xbuf.at[j, core, q], tsend.at[0], trecv.at[j], partner
         )
 
     def select(j):
@@ -575,7 +575,7 @@
         return remote(
             ybuf.at[j, 1 - core, :, :, columns],
             yin.at[j, :, :, columns],
-            ysend.at[j, h],
+            ysend.at[0],
             yrecv.at[j, h],
             partner,
         )
@@ -611,8 +611,8 @@
         return remote(
             sbuf.at[j, q, :, columns],
             rbuf.at[j, p, :, columns],
-            rsend.at[j, i, h],
-            rrecv.at[j, i, h],
+            rsend.at[0],
+            rrecv.at[j, h],
             at(z, q),
         )
 
@@ -627,11 +627,12 @@
 
     def chain_copy(way, block, part, target):
         columns = pl.ds(part * chain_width, chain_width)
+        lane_of = jnp.where((way == 1) & (block == target), line, block)
         return remote(
             csend.at[block, :, columns],
-            pin.at[way, block, :, columns],
-            ssend.at[block, part],
-            srecv.at[way, block, part],
+            pin.at[lane_of, :, columns],
+            ssend.at[0],
+            srecv.at[lane_of, part],
             at(target, p),
         )
 
@@ -645,8 +646,7 @@
         return high, (weigh - high.astype(f32)).astype(bf16)
 
     def combine(j, h, weigh):
-        for i in range(1, plane):
-            return_copy(j, i, h).wait_recv()
+        came(rbuf.at[j, others, :, pl.ds(h * half, half)], rrecv.at[j, h])
         block = block_of(j)
         high, low = weigh
         columns = pl.ds(h * half, half)
@@ -684,7 +684,7 @@
         @pl.when(inside)
         def _():
             chain_copy(way, block, part, z).wait_recv()
-            total = cbuf[block, :, columns] + pin[way, block, :, columns].astype(f32)
+            total = cbuf[block, :, columns] + pin[block, :, columns].astype(f32)
             csend[block, :, columns] = total.astype(bf16)
             chain_copy(way, block, part, z + 1 - 2 * way).start()
 
@@ -706,18 +706,16 @@
     with sc("select#0"):
         select(0)
     with sc("meta"):
-        for i in range(1, line):
-            meta_copy(i).wait_recv()
+        came(meta.at[pl.ds(0, line - 1)], mrecv.at[0])
     with sc("pass#1a"):
         pass_on(1, 0, parts // 2)
     with sc("collect#0"):
         collect(0)
     for j in range(line):
         last = j + 1 == line
-        cut = tiles if last else (tiles + j) // 2
+        cut = tiles if last else tiles // 2 if j == 0 else 0
         with sc(f"xwait#{j}"):
-            for i in range(plane):
-                partner_copy(j, i).wait_recv()
+            came(xbuf.at[j, 1 - core], trecv.at[j])
             if j == 0:
                 for copy in weights:
                     copy.wait()
@@ -730,18 +728,13 @@
                 select(j + 1)
         with sc(f"widen#{j}b"):
             widen(j, cut, tiles)
-        if j >= 2 and last:
+        if j >= 2:
             with sc(f"combine#{j - 1}"):
                 weigh = weigh_of(j - 1)
                 for h in range(halves):
                     combine(j - 1, h, weigh)
         with sc(f"narrow#{j}a"):
             narrow(j, 0)
-        if j >= 2 and not last:
-            with sc(f"combine#{j - 1}"):
-                weigh = weigh_of(j - 1)
-                for h in range(halves):
-                    combine(j - 1, h, weigh)
         with sc(f"narrow#{j}b"):
             for h in range(1, halves):
                 narrow(j, h)
@@ -778,6 +771,12 @@
         weigh = weigh_of(0)
         for h in range(halves):
             combine(0, h, weigh)
+    def out_copy(part):
+        columns = pl.ds(part * chain_width, chain_width)
+        return pltpu.make_async_copy(
+            got_ref.at[:, columns], out_ref.at[:, columns], osem.at[0]
+        )
+
     with sc("own"):
         for part in range(chain):
             columns = pl.ds(part * chain_width, chain_width)
@@ -785,56 +784,40 @@
             @pl.when(z > 0)
             def _():
                 chain_copy(0, z, part, z).wait_recv()
-                cbuf[z, :, columns] = cbuf[z, :, columns] + pin[0, z, :, columns].astype(f32)
+                cbuf[z, :, columns] = cbuf[z, :, columns] + pin[z, :, columns].astype(f32)
 
             @pl.when(z < line - 1)
             def _():
                 chain_copy(1, z, part, z).wait_recv()
-                cbuf[z, :, columns] = cbuf[z, :, columns] + pin[1, z, :, columns].astype(f32)
-
-    out_ref[...] = cbuf[z].astype(bf16)
-
-    for i in range(1, line):
-        meta_copy(i).wait_send()
-
-        @pl.when(z + i < line)
-        def _():
-            line_state_copy(i).wait_send()
-            line_total_copy(i).wait_send()
-
-    for i in range(1, plane):
-        state_copy(i).wait_send()
-        total_copy(i).wait_send()
-        start_copy(i).wait_send()
-    for h in range(2):
-        away_copy(h).wait_send()
-    for part in range(parts):
-        for block in range(line):
-
-            @pl.when((z >= block) & (z + 1 < line))
+                cbuf[z, :, columns] = cbuf[z, :, columns] + pin[line, :, columns].astype(f32)
+
+            got_ref[:, columns] = cbuf[z, :, columns].astype(bf16)
+            out_copy(part).start()
+
+    with sc("store"):
+        pltpu.make_async_copy(got_ref, out_ref, osem.at[0]).wait()
+
+    with sc("drain"):
+        sent(meta.at[pl.ds(0, line - 1)], msend.at[0])
+        sent(state_out.at[others], asend.at[0])
+        sent(totals.at[others], bsend.at[0])
+        sent(back_state.at[others], dsend.at[0])
+        sent(away_ref, esend.at[0])
+        sent(sel.at[:, others], psend.at[0])
+        sent(sel, tsend.at[0])
+        sent(yin, ysend.at[0])
+        sent(sbuf.at[:, others], rsend.at[0])
+        sent(csend.at[pl.ds(0, line - 1)], ssend.at[0])
+        for place in range(line):
+
+            @pl.when(z == place)
             def _():
-                row_copy(0, block, part, z).wait_send()
-
-            @pl.when((z <= block) & (z > 0))
-            def _():
-                row_copy(1, block, part, z).wait_send()
-
-    for part in range(chain):
-        for block in range(line):
-
-            @pl.when(z != block)
-            def _():
-                chain_copy(0, block, part, z).wait_send()
-
-    for j in range(line):
-        for i in range(1, plane):
-            select_copy(j, i).wait_send()
-        for i in range(plane):
-            partner_copy(j, i).wait_send()
-        for h in range(halves):
-            partial_copy(j, h).wait_send()
-            for i in range(1, plane):
-                return_copy(j, i, h).wait_send()
+                if place + 1 < line:
+                    sent(zbuf.at[pl.ds(0, place + 1)], zsend.at[0])
+                    sent(line_state.at[pl.ds(0, line - 1 - place)], ctsend.at[0])
+                    sent(line_total.at[pl.ds(0, line - 1 - place)], ctsend.at[1])
+                if place > 0:
+                    sent(zbuf.at[pl.ds(place, line - place)], zsend.at[1])
 
 
 def run_layer(inputs, small, weights, cap):
@@ -852,7 +835,7 @@
     slice_rows = groups * size // plane
     inner = weights[0].shape[2]
     slots = plane * cap
-    parts, halves, chain = 2, 2, 4
+    parts, halves, chain = 2, 2, 8
     bf16, f32 = jnp.bfloat16, jnp.float32
     dma = pltpu.SemaphoreType.DMA
     vmem = pl.BlockSpec(memory_space=pltpu.VMEM)
@@ -861,7 +844,7 @@
         functools.partial(layer_kernel, line, plane, cap, parts, halves, chain),
         out_shape=jax.ShapeDtypeStruct((tokens, width), bf16),
         in_specs=[hbm] * 4 + [vmem] * 2 + [hbm] * 2 + [vmem] * 3 + [hbm] * 3,
-        out_specs=vmem,
+        out_specs=hbm,
         scratch_shapes=[
             pltpu.VMEM((length, channels), bf16),
             pltpu.VMEM((length, channels), bf16),
@@ -894,15 +877,16 @@
             pltpu.VMEM((plane, slice_rows, lanes), bf16),
             pltpu.VMEM((plane, slice_rows, lanes), bf16),
             dma((6,)),
-            dma((plane,)),
-            dma((plane,)),
-            dma((plane,)),
-            dma((plane,)),
+            dma((1,)),
+            dma((1,)),
+            dma((1,)),
+            dma((1,)),
+            dma((1,)),
+            dma((2,)),
             dma((line, 2)),
-            dma((line, 2)),
-            dma((plane,)),
-            dma((plane,)),
-            dma((2,)),
+            dma((1,)),
+            dma((1,)),
+            dma((1,)),
             dma((2,)),
             pltpu.VMEM((width, inner), bf16),
             pltpu.VMEM((width, inner), bf16),
@@ -918,22 +902,22 @@
             pltpu.VMEM((line, plane, cap, width), bf16),
             pltpu.VMEM((line, tokens, width), f32),
             pltpu.VMEM((line, tokens, width), bf16),
-            pltpu.VMEM((2, line, tokens, width), bf16),
-            dma((3, 4)),
-            dma((2, line, parts)),
+            pltpu.VMEM((line + 1, tokens, width), bf16),
+            dma((3,)),
+            dma((2,)),
             dma((line, parts)),
+            dma((1,)),
+            dma((1,)),
+            dma((1,)),
+            dma((line, plane)),
+            dma((1,)),
             dma((line,)),
-            dma((line,)),
-            dma((line, plane)),
-            dma((line, plane)),
-            dma((line, plane)),
-            dma((line, plane)),
+            dma((1,)),
             dma((line, halves)),
+            dma((1,)),
             dma((line, halves)),
-            dma((line, plane, halves)),
-            dma((line, plane, halves)),
-            dma((line, chain)),
-            dma((2, line, chain)),
+            dma((1,)),
+            dma((line + 1, chain)),
         ],
         compiler_params=pltpu.CompilerParams(
             collective_id=1, has_side_effects=True, vmem_limit_bytes=67043328

time: 111 us -> 108 us (0.973)
  Pallas kernels: 109 us -> 106 us
    pallas_call x1, Pallas kernels: 109 us -> 106 us  [run_layer(): pl.pallas_call(functools.partial(layer_kernel, line, plane, cap, parts, h...]
where the time goes in v4:
time: 108 us; the launch traced here: 107 us
  Pallas kernels  106 us (98%)
  local copies, waits for them, and re-layouts  1.88 us (2%)
    pallas_call x1, Pallas kernels, run_layer(): pl.pallas_call(functools.partial(layer_kernel, line, plane, cap, parts, h...  106 us

profile of v4, /device:TPU:0, one launch (start us, length us, event | category | flops | bytes accessed | tf_op | source)
XLA Modules:
  0.0 107.5 jit_solution(4227642851902648501)
XLA Ops:
  0.0 105.6 %layer.1 = bf16[128,2048]{1,0:T(8,128)(2,1)} custom-call(bf16[256,512]{1,0:T(8,128)(2,1)} %query_hbm.1, bf16[256,512]{1,0:T(8,128)(2,1)} %key_hbm.1, bf16[256,512]{1,0:T(8,128)(2,1)} %value_hbm.1, bf16[256,512]{1,0:T(8,128)(2,1)} %gates_hbm.1, f32[8,256]{1,0:T(8,128)} %bitcast.5, f32[1,512]{1,0:T(1,128)} %bitcast.7, bf16[512,2048]{1,0:T(8,128)(2,1)} %project_hbm.1, ...), custom_call_target="tpu_custom_call" | custom-call | tf_op jit(solution)/shard_map/layer/pallas_call | solution.py:843
  105.6 1.9 %copy.16 = bf16[128,2048]{1,0:T(8,128)(2,1)} copy(bf16[128,2048]{1,0:T(8,128)(2,1)} %layer.1) | data formatting | bytes 1048576

commit v5 on v4

--- a/solution.py
+++ b/solution.py
@@ -28,17 +28,22 @@
     key_hbm,
     value_hbm,
     gates_hbm,
-    decay_ref,
-    gain_ref,
+    decay_hbm,
+    gain_hbm,
     project_hbm,
     residual_hbm,
-    norm_ref,
-    ids_ref,
-    shares_ref,
+    norm_hbm,
+    ids_hbm,
+    shares_hbm,
     gate_hbm,
     up_hbm,
     down_hbm,
     out_ref,
+    decay_ref,
+    gain_ref,
+    norm_ref,
+    ids_ref,
+    shares_ref,
     query_ref,
     key_ref,
     value_ref,
@@ -151,12 +156,17 @@
         pltpu.make_async_copy(source, target, lsem.at[number])
         for number, (source, target) in enumerate(
             (
+                (decay_hbm, decay_ref),
+                (ids_hbm, ids_ref),
+                (shares_hbm, shares_ref),
                 (query_hbm, query_ref),
                 (key_hbm, key_ref),
                 (value_hbm, value_ref),
                 (gates_hbm, gates_ref),
                 (project_hbm, project_ref),
                 (residual_hbm, residual_ref),
+                (gain_hbm, gain_ref),
+                (norm_hbm, norm_ref),
             )
         )
     ]
@@ -191,32 +201,6 @@
             value = jnp.where(lane < (number + 1) * size, pieces[number], value)
         return value
 
-    with jax.named_scope("running"):
-        rows_of = lax.broadcasted_iota(jnp.int32, (length, length), 0)
-        columns_of = lax.broadcasted_iota(jnp.int32, (length, length), 1)
-        causal = rows_of >= columns_of
-        lower = jnp.where(causal, 1.0, 0.0).astype(bf16)
-        upper = jnp.where(rows_of <= columns_of, 1.0, 0.0).astype(bf16)
-        spread = lax.broadcasted_iota(jnp.int32, (heads, channels), 1) // size == (
-            lax.broadcasted_iota(jnp.int32, (heads, channels), 0)
-        )
-        spread = jnp.where(spread, 1.0, 0.0).astype(bf16)
-        rest = decay_ref[...]
-        running, by_head = 0.0, 0.0
-        for _ in range(3):
-            piece = rest.astype(bf16)
-            rest = rest - piece.astype(f32)
-            wide_piece = lax.dot_general(piece, spread, upright, preferred_element_type=f32)
-            wide_piece = wide_piece.astype(bf16)
-            running = running + jnp.dot(lower, wide_piece, preferred_element_type=f32)
-            by_head = by_head + jnp.dot(piece, upper, preferred_element_type=f32)
-        running_ref[...] = running
-        by_head_ref[...] = by_head
-
-    swapped = lax.broadcasted_iota(jnp.int32, (lanes, lanes), 0) == (
-        lax.broadcasted_iota(jnp.int32, (lanes, lanes), 1) ^ (size // 2)
-    )
-    swapped = jnp.where(swapped, 1.0, 0.0).astype(bf16)
     with jax.named_scope("table"):
         half_size = size // 2
         step_of = lane % half_size
@@ -239,8 +223,37 @@
             cos_ref[some, :] = a * near_cos - b * near_sin
             sin_ref[some, :] = (b * near_cos + a * near_sin) * sign
 
+    for copy in loads[:3]:
+        copy.wait()
+
+    with jax.named_scope("running"):
+        rows_of = lax.broadcasted_iota(jnp.int32, (length, length), 0)
+        columns_of = lax.broadcasted_iota(jnp.int32, (length, length), 1)
+        causal = rows_of >= columns_of
+        lower = jnp.where(causal, 1.0, 0.0).astype(bf16)
+        upper = jnp.where(rows_of <= columns_of, 1.0, 0.0).astype(bf16)
+        spread = lax.broadcasted_iota(jnp.int32, (heads, channels), 1) // size == (
+            lax.broadcasted_iota(jnp.int32, (heads, channels), 0)
+        )
+        spread = jnp.where(spread, 1.0, 0.0).astype(bf16)
+        rest = decay_ref[...]
+        running, by_head = 0.0, 0.0
+        for _ in range(3):
+            piece = rest.astype(bf16)
+            rest = rest - piece.astype(f32)
+            wide_piece = lax.dot_general(piece, spread, upright, preferred_element_type=f32)
+            wide_piece = wide_piece.astype(bf16)
+            running = running + jnp.dot(lower, wide_piece, preferred_element_type=f32)
+            by_head = by_head + jnp.dot(piece, upper, preferred_element_type=f32)
+        running_ref[...] = running
+        by_head_ref[...] = by_head
+
+    swapped = lax.broadcasted_iota(jnp.int32, (lanes, lanes), 0) == (
+        lax.broadcasted_iota(jnp.int32, (lanes, lanes), 1) ^ (size // 2)
+    )
+    swapped = jnp.where(swapped, 1.0, 0.0).astype(bf16)
     with jax.named_scope("loadw"):
-        for copy in loads[:3]:
+        for copy in loads[3:6]:
             copy.wait()
 
     def turn(block):
@@ -408,7 +421,7 @@
         start_copy(i).start()
     start_state[p] = back_state[p]
     with jax.named_scope("wait3"):
-        for copy in loads[3:]:
+        for copy in loads[6:]:
             copy.wait()
         came(start_state.at[others], drecv.at[0])
 
@@ -835,17 +848,21 @@
     slice_rows = groups * size // plane
     inner = weights[0].shape[2]
     slots = plane * cap
-    parts, halves, chain = 2, 2, 8
+    parts, halves, chain = 2, 2, 16
     bf16, f32 = jnp.bfloat16, jnp.float32
     dma = pltpu.SemaphoreType.DMA
-    vmem = pl.BlockSpec(memory_space=pltpu.VMEM)
     hbm = pl.BlockSpec(memory_space=pl.ANY)
     return pl.pallas_call(
         functools.partial(layer_kernel, line, plane, cap, parts, halves, chain),
         out_shape=jax.ShapeDtypeStruct((tokens, width), bf16),
-        in_specs=[hbm] * 4 + [vmem] * 2 + [hbm] * 2 + [vmem] * 3 + [hbm] * 3,
+        in_specs=[hbm] * 14,
         out_specs=hbm,
         scratch_shapes=[
+            pltpu.VMEM(decay.shape, decay.dtype),
+            pltpu.VMEM(gain.shape, gain.dtype),
+            pltpu.VMEM(norm.shape, norm.dtype),
+            pltpu.VMEM(ids.shape, ids.dtype),
+            pltpu.VMEM(shares.shape, shares.dtype),
             pltpu.VMEM((length, channels), bf16),
             pltpu.VMEM((length, channels), bf16),
             pltpu.VMEM((length, channels), bf16),
@@ -876,7 +893,7 @@
             pltpu.VMEM((slice_rows, lanes), f32),
             pltpu.VMEM((plane, slice_rows, lanes), bf16),
             pltpu.VMEM((plane, slice_rows, lanes), bf16),
-            dma((6,)),
+            dma((11,)),
             dma((1,)),
             dma((1,)),
             dma((1,)),

time: 108 us -> 107 us (level)
  no operation moved by 1% of the time
where the time goes in v5:
time: 107 us
  Pallas kernels  105 us (98%)
  local copies, waits for them, and re-layouts  1.88 us (2%)
    pallas_call x1, Pallas kernels, run_layer(): pl.pallas_call(functools.partial(layer_kernel, line, plane, cap, parts, h...  105 us

profile of v5, /device:TPU:0, one launch (start us, length us, event | category | flops | bytes accessed | tf_op | source)
XLA Modules:
  0.0 106.6 jit_solution(1886111825770687377)
XLA Ops:
  0.0 104.7 %layer.1 = bf16[128,2048]{1,0:T(8,128)(2,1)} custom-call(bf16[256,512]{1,0:T(8,128)(2,1)} %query_hbm.1, bf16[256,512]{1,0:T(8,128)(2,1)} %key_hbm.1, bf16[256,512]{1,0:T(8,128)(2,1)} %value_hbm.1, bf16[256,512]{1,0:T(8,128)(2,1)} %gates_hbm.1, f32[8,256]{1,0:T(8,128)} %bitcast.5, f32[1,512]{1,0:T(1,128)} %bitcast.7, bf16[512,2048]{1,0:T(8,128)(2,1)} %project_hbm.1, ...), custom_call_target="tpu_custom_call" | custom-call | tf_op jit(solution)/shard_map/layer/pallas_call | solution.py:855
  104.7 1.9 %copy.16 = bf16[128,2048]{1,0:T(8,128)(2,1)} copy(bf16[128,2048]{1,0:T(8,128)(2,1)} %layer.1) | data formatting | bytes 1048576
